TPU v7x, 256 devices: a 8x8x2 block of a 8x8x16 slice. The times are simulated.
256 devices in a mesh: grp: 2 (over z), sp: 16 (over y, core), tp: 8 (over x).
Axes of the slice: x: 8, y: 8, z: 2, core: 2. Of those that a mesh axis runs over, the one named last changes fastest.
The devices are a block of a 8x8x16 slice.
Arguments:
- residual: bfloat16 [3072, 8, 2048], P(('sp', 'tp'), 'grp'), parts along dimension 1, may hold values from -6 to 6
- query: bfloat16 [3072, 8, 1536], P('sp', 'grp', 'tp'), parts along dimension 1, may hold values from -64 to 64
- latent: bfloat16 [3072, 8, 512], P('sp', 'grp'), parts along dimension 1, may hold values from -6 to 6
- rope_key: bfloat16 [3072, 8, 64], P('sp', 'grp'), parts along dimension 1, may hold values from -8 to 8
- latent_gain: float32 [512], replicated, may hold values from 0.1 to 1.9
- key_up: bfloat16 [512, 1024], P(None, 'tp'), may hold values from -0.25 to 0.25
- value_up: bfloat16 [512, 1024], P(None, 'tp'), may hold values from -0.25 to 0.25
- out_weight: bfloat16 [1024, 2048], P('tp'), may hold values from -0.375 to 0.375
- norm_gain: float32 [2048], replicated, may hold values from 0.1 to 1.9
- group_prob: float32 [3072, 8], P(('sp', 'tp'), 'grp'), parts along dimension 1, may hold values from 0.25 to 1
- pair_logits: float32 [3072, 8, 2], P(('sp', 'tp'), 'grp'), parts along dimension 1, may hold values from -8 to 8
- routes: int32 [3072, 8, 2], P(('sp', 'tp'), 'grp'), parts along dimension 1, may hold values from 0 to 127, all different within a row; in each aligned block of 96 rows (0 to 95, 96 to 191, ..., all dimensions but the last counted through in order) at most 2 rows name the same one
- w_gate: bfloat16 [128, 2048, 768], P(('sp', 'tp')), may hold values from -0.125 to 0.125
- w_up: bfloat16 [128, 2048, 768], P(('sp', 'tp')), may hold values from -0.125 to 0.125
- w_down: bfloat16 [128, 768, 2048], P(('sp', 'tp')), may hold values from -0.4375 to 0.4375
Outputs:
- layer_out: bfloat16 [3072, 8, 2048], P(('sp', 'tp'), 'grp'), parts along dimension 1
There are 2 independent parts, one for each index of `grp`. A program takes and returns all parts, laid end to end along the dimension named above; an argument that names none is the same for every part. Nothing has to cross between parts.
Inputs may be any that keep to these rules, and one draw needn't show every extreme that they name: `routes`: A token's 2 experts differ. Among the tokens of one device (aligned blocks of 96 rows in position-then-sequence order), no expert is named more than 2 times, a bound that some block reaches.
All inputs are finite; a program needn't handle non-finite values.
Results may differ from a plain program's by a relative error of at most 0.013.
Values may be sent and summed in bfloat16 or wider, within the bound.
A program may use at most 128 MiB of HBM per device.

v0:
```python
import math

import jax
import jax.numpy as jnp
from jax import lax
from jax.sharding import PartitionSpec as P

D = 2048
NOPE = 128
VDIM = 128
QK = 192
TOPK = 2
SEQS = 4


epsilon = 1e-06
rotary_base = 10000.0
lowest = -1e30


def side_by_side(arrays, axis, dim, along):
    widths = [math.prod(a.shape[along:]) for a in arrays]
    both = jnp.concatenate(
        [a.reshape(*a.shape[:along], w) for a, w in zip(arrays, widths)], axis=along
    )
    out = lax.all_gather(both, axis, axis=dim, tiled=True)
    pieces = jnp.split(out, [sum(widths[:k]) for k in range(1, len(widths))], axis=along)
    return tuple((b.reshape(*out.shape[:along], *a.shape[along:]) for a, b in zip(arrays, pieces)))


def in_blocks(shard, dim, peers):
    dims = shard.shape
    pieces = shard.reshape(*dims[:dim], peers, dims[dim] // peers, *dims[dim + 1 :])
    return jnp.moveaxis(pieces, dim, 0)


def laid_out(pieces, dim):
    pieces = jnp.moveaxis(pieces, 0, dim)
    dims = pieces.shape
    return pieces.reshape(*dims[:dim], dims[dim] * dims[dim + 1], *dims[dim + 2 :])


def joined_exchange(shard, axis, axes, splits, concats):
    sizes = [lax.axis_size(a) for a in axes]
    pieces = in_blocks(shard, splits[0], sizes[0])
    pieces = jnp.moveaxis(in_blocks(pieces, splits[1] + 1, sizes[1]), 0, 1)
    inside = pieces.shape[2:]
    pieces = pieces.reshape(-1, *inside)
    pieces = lax.all_to_all(pieces, axis, split_axis=0, concat_axis=0, tiled=True)
    pieces = laid_out(pieces.reshape(*sizes, *inside), concats[0] + 1)
    return laid_out(pieces, concats[1])


def rotate(values, positions):
    halfway = values.shape[-1] // 2
    inverse = rotary_base ** (-jnp.arange(halfway, dtype=jnp.float32) / halfway)
    angles = positions.astype(jnp.float32)[:, None] * inverse[None, :]
    angles = angles.reshape((angles.shape[0],) + (1,) * (values.ndim - 2) + (halfway,))
    cosine_values = jnp.cos(angles)
    sine_values = jnp.sin(angles)
    first_half = values[..., :halfway]
    second_half = values[..., halfway:]
    return jnp.concatenate(
        [
            first_half * cosine_values - second_half * sine_values,
            second_half * cosine_values + first_half * sine_values,
        ],
        axis=-1,
    )


def rms_scale(values, gain_values):
    return (
        values
        * lax.rsqrt(jnp.mean(values * values, axis=-1, keepdims=True) + epsilon)
        * gain_values
    )


def expand(latent_rows, latent_gain, key_up, value_up):
    normed = rms_scale(latent_rows.astype(jnp.float32), latent_gain).astype(jnp.bfloat16)
    keys_nope = jnp.dot(normed, key_up, preferred_element_type=jnp.float32).astype(jnp.bfloat16)
    values = jnp.dot(normed, value_up, preferred_element_type=jnp.float32).astype(jnp.bfloat16)
    lead = latent_rows.shape[:2]
    return (
        keys_nope.reshape(lead + (key_up.shape[1] // NOPE, NOPE)),
        values.reshape(lead + (value_up.shape[1] // VDIM, VDIM)),
    )


def absorb(carried, query_nope, query_rot, key_nope, value_rows, key_rot):
    running, totals, accumulated = carried
    scores = jnp.einsum("qshd,kshd->qshk", query_nope, key_nope, preferred_element_type=jnp.float32)
    scores = scores + jnp.einsum(
        "qshd,ksd->qshk", query_rot, key_rot, preferred_element_type=jnp.float32
    )
    scores = scores * QK ** (-0.5)
    highest = jnp.maximum(running, jnp.max(scores, axis=-1))
    weights = jnp.exp(scores - highest[..., None])
    totals = jnp.sum(weights, axis=-1)
    accumulated = jnp.einsum(
        "qshk,kshd->qshd",
        weights.astype(jnp.bfloat16),
        value_rows,
        preferred_element_type=jnp.float32,
    )
    return (highest, totals, accumulated)


def shards(
    residual,
    query,
    latent,
    rope_key,
    latent_gain,
    key_up,
    value_up,
    out_weight,
    norm_gain,
    group_prob,
    pair_logits,
    routes,
    w_gate,
    w_up,
    w_down,
):
    positions_here = query.shape[0]
    heads_here = key_up.shape[1] // NOPE
    own_positions = lax.axis_index("sp") * positions_here + jnp.arange(
        positions_here, dtype=jnp.int32
    )
    split_query = query.reshape(positions_here, SEQS, heads_here, QK)
    query_nope = split_query[..., :NOPE]
    query_rot = rotate(split_query[..., NOPE:].astype(jnp.float32), own_positions).astype(
        jnp.bfloat16
    )
    key_rot = rotate(rope_key.astype(jnp.float32), own_positions).astype(jnp.bfloat16)
    initial = (
        jnp.full((positions_here, SEQS, heads_here), lowest, jnp.float32),
        jnp.zeros((positions_here, SEQS, heads_here), jnp.float32),
        jnp.zeros((positions_here, SEQS, heads_here, VDIM), jnp.float32),
    )
    own_keys, own_values = expand(latent, latent_gain, key_up, value_up)
    pieces = side_by_side((own_keys, own_values, key_rot), "sp", 0, 2)
    finished = absorb(initial, query_nope, query_rot, pieces[0], pieces[1], pieces[2])
    attended = (finished[2] / finished[1][..., None]).astype(jnp.bfloat16)
    attended = attended.reshape(positions_here, SEQS, heads_here * VDIM)
    by_token = lax.all_to_all(attended, "tp", split_axis=0, concat_axis=2, tiled=True)
    row_count = by_token.shape[0] * SEQS
    mixed_heads = by_token.reshape(row_count, by_token.shape[2])
    projected = jnp.dot(
        mixed_heads,
        lax.all_gather(out_weight, "tp", axis=0, tiled=True),
        preferred_element_type=jnp.float32,
    )
    stream = (residual.reshape(row_count, D).astype(jnp.float32) + projected).astype(jnp.bfloat16)
    normed = rms_scale(stream.astype(jnp.float32), norm_gain).astype(jnp.bfloat16)
    mixing = jax.nn.softmax(pair_logits.reshape(row_count, TOPK), axis=-1) * group_prob.reshape(
        row_count, 1
    )
    experts_total = lax.axis_size("sp") * lax.axis_size("tp")
    capacity = max(2, 3 * row_count * TOPK // (2 * experts_total))
    pick_count = row_count * TOPK
    chosen = routes.reshape(pick_count)
    one_hot = (chosen[:, None] == jnp.arange(experts_total, dtype=jnp.int32)[None, :]).astype(
        jnp.bfloat16
    )
    earlier = (jnp.arange(pick_count)[:, None] > jnp.arange(pick_count)[None, :]).astype(
        jnp.bfloat16
    )
    before = jnp.dot(earlier, one_hot, preferred_element_type=jnp.float32)
    slot_index = jnp.sum(before * one_hot.astype(jnp.float32), axis=-1).astype(jnp.int32)
    target = chosen * capacity + slot_index
    source_row = (
        jnp.full((experts_total * capacity,), row_count, jnp.int32)
        .at[target]
        .set(jnp.arange(pick_count, dtype=jnp.int32) // TOPK)
    )
    padded = jnp.concatenate([normed, jnp.zeros((1, D), jnp.bfloat16)], axis=0)
    outgoing = padded[source_row].reshape(experts_total, capacity, D)
    sectioned = outgoing.reshape(lax.axis_size("sp"), lax.axis_size("tp"), capacity, D)
    arrived = joined_exchange(sectioned, ("sp", "tp"), ("sp", "tp"), (0, 1), (0, 1))
    flat_rows = arrived.reshape(-1, D)
    gate_pre = jnp.dot(flat_rows, w_gate[0], preferred_element_type=jnp.float32)
    upward = jnp.dot(flat_rows, w_up[0], preferred_element_type=jnp.float32)
    hidden = (jax.nn.silu(gate_pre) * upward).astype(jnp.bfloat16)
    returned = joined_exchange(
        jnp.dot(hidden, w_down[0], preferred_element_type=jnp.float32)
        .astype(jnp.bfloat16)
        .reshape(arrived.shape),
        ("sp", "tp"),
        ("sp", "tp"),
        (0, 1),
        (0, 1),
    )
    results = returned.reshape(experts_total * capacity, D)[target].reshape(row_count, TOPK, D)
    combined = stream.astype(jnp.float32) + jnp.sum(
        results.astype(jnp.float32) * mixing[..., None], axis=1
    )
    return combined.astype(jnp.bfloat16).reshape(residual.shape)


def solution(mesh):
    placed = (
        P(("sp", "tp"), "grp", None),
        P("sp", "grp", "tp"),
        P("sp", "grp", None),
        P("sp", "grp", None),
        P(),
        P(None, "tp"),
        P(None, "tp"),
        P("tp", None),
        P(),
        P(("sp", "tp"), "grp"),
        P(("sp", "tp"), "grp", None),
        P(("sp", "tp"), "grp", None),
        P(("sp", "tp"), None, None),
        P(("sp", "tp"), None, None),
        P(("sp", "tp"), None, None),
    )
    return jax.shard_map(
        shards, mesh=mesh, in_specs=placed, out_specs=P(("sp", "tp"), "grp", None), check_vma=False
    )
```

profile of v0, /device:TPU:513, one launch (start us, length us, event | category | flops | bytes accessed | tf_op | source)
XLA Modules:
  0.0 285.6 jit_solution(10172775270289850138)
XLA Ops:
  7.9 1.6 fusion.22
  19.7 1.9 fusion.57
  21.6 74.0 %all-gather.3.cloned.1.call-done = bf16[3072,4,320]{2,0,1:T(8,128)(2,1)} async-done(((bf16[192,4,320]{2,0,1:T(8,128)(2,1)}), bf16[3072,4,320]{2,0,1:T(8,128)(2,1)}) %all-gather.3.cloned.1.call-update) | async-done | bytes 7864336 | tf_op jit(solution)/shard_map/all_gather | solution.py:26
  95.6 3.3 %fusion.9 = f32[4,3072,192]{1,2,0:T(8,128)S(1)} fusion(bf16[3072,4,320]{2,0,1:T(8,128)(2,1)} %all-gather.3.cloned.1.call-done, bf16[192,4,1,192]{3,0,1,2:T(8,128)(2,1)S(1)} %bitcast.106), kind=kOutput, calls=%fused_computation.13 | convolution fusion | flops 603979776 | bytes 12779520 | tf_op jit(solution)/shard_map/qshd,kshd->qshk/dot_general | solution.py:93
  98.9 3.3 %fusion.72 = (f32[192,4]{0,1:T(4,128)S(1)}, f32[192,4,1,3072]{3,0,1,2:T(8,128)S(1)}) fusion(bf16[192,4,32]{2,0,1:T(8,128)(2,1)S(1)} %copy-done.5, bf16[192,4,32]{2,0,1:T(8,128)(2,1)S(1)} %copy-done.4, bf16[3072,4,320]{2,0,1:T(8,128)(2,1)} %all-gather.3.cloned.1.call-done, f32[4,3072,192]{1,2,0:T(8,128)S(1)} %fusion.9), kind=kOutput, calls=%fused_computation.90 | convolution fusion | flops 309263616 | bytes 22121472 | tf_op jit(solution)/shard_map/qshd,ksd->qshk/dot_general | solution.py:94
  103.7 3.6 %fusion.47 = bf16[192,4,128]{2,0,1:T(8,128)(2,1)S(1)} fusion(bf16[3072,4,320]{2,0,1:T(8,128)(2,1)} %all-gather.3.cloned.1.call-done, f32[192,4,1,3072]{3,0,1,2:T(8,128)S(1)} %get-tuple-element.12, f32[192,4]{0,1:T(4,128)S(1)} %broadcast_maximum_fusion, f32[192,4]{0,1:T(4,128)S(1)} %fusion.1), kind=kOutput, calls=%fused_computation.40 | convolution fusion | flops 608894976 | bytes 12785664 | tf_op jit(solution)/shard_map/qshk,kshd->qshd/dot_general | solution.py:101
  108.2 6.4 %all-to-all-start = ((bf16[192,4,128]{2,1,0:T(4,128)(2,1)}), bf16[192,4,128]{2,1,0:T(4,128)(2,1)S(1)}, u32[]{:S(2)}, u32[]{:S(2)}) async-start(bf16[192,4,128]{2,1,0:T(4,128)(2,1)} %copy.80), calls=%async_computation | async-start | bytes 393216 | tf_op jit(solution)/shard_map/all_to_all | solution.py:148
  114.6 1.9 reshape.327
  117.9 9.5 %all-to-all-done = bf16[192,4,128]{2,1,0:T(4,128)(2,1)S(1)} async-done(((bf16[192,4,128]{2,1,0:T(4,128)(2,1)}), bf16[192,4,128]{2,1,0:T(4,128)(2,1)S(1)}, u32[]{:S(2)}, u32[]{:S(2)}) %all-to-all-start) | async-done | bytes 196640 | tf_op jit(solution)/shard_map/all_to_all | solution.py:148
  127.6 27.8 %all-gather.5.cloned.1.call-done = bf16[1024,2048]{1,0:T(8,128)(2,1)} async-done(((bf16[128,2048]{1,0:T(8,128)(2,1)}), bf16[1024,2048]{1,0:T(8,128)(2,1)}) %all-gather.5.cloned.1.call-update) | async-done | bytes 4194320 | tf_op jit(solution)/shard_map/all_gather | solution.py:153
  155.4 3.3 %multiply_reduce_fusion.1 = (f32[96]{0:T(128)S(1)}, f32[96,2048]{1,0:T(8,128)S(1)}) fusion(f32[96,2048]{1,0:T(8,128)} %reshape.327, bf16[1024,2048]{1,0:T(8,128)(2,1)} %all-gather.5.cloned.1.call-done, bf16[12,8,8,128]{3,2,1,0:T(8,128)(2,1)S(1)} %bitcast.107), kind=kOutput, calls=%fused_computation.43 | convolution fusion | flops 403636128 | bytes 5964160 | tf_op jit(solution)/shard_map/dot_general | solution.py:151
  160.5 4.4 %gather_fusion = bf16[256,2048]{1,0:T(8,128)(2,1)} fusion(bf16[97,2048]{1,0:T(8,128)(2,1)} %concatenate.24, s32[1024]{0:T(1024)S(1)} %pad_clamp_fusion.1), kind=kCustom, calls=%fused_computation | custom fusion | bytes 2098176 | tf_op jit(solution)/shard_map/gather | solution.py:180
  164.9 2.5 reshape_transpose_transpose_reshape_reshape_reshape_reshape.3
  167.4 42.9 %all_to_all.25 = bf16[128,1,1,2,2048]{4,3,2,1,0:T(2,128)(2,1)} all-to-all(bf16[128,1,1,2,2048]{4,3,2,1,0:T(2,128)(2,1)} %bitcast.103), channel_id=1, replica_groups=mesh['grp'=2,'sp'=16,'tp'=8] {'sp','tp'}, dimensions={0} | all-to-all | bytes 2097152 | tf_op jit(solution)/shard_map/all_to_all | solution.py:49
  210.3 2.2 reshape_reshape.6
  212.6 4.1 %fusion.15 = f32[256,768]{1,0:T(8,128)} fusion(bf16[256,2048]{1,0:T(8,128)(2,1)} %reshape_reshape.6, bf16[1,2048,768]{2,1,0:T(8,128)(2,1)} %param.27), kind=kOutput, calls=%fused_computation.19 | convolution fusion | flops 805306368 | bytes 4980736 | tf_op jit(solution)/shard_map/dot_general | solution.py:184
  216.7 5.5 %fusion.17 = bf16[256,2048]{1,0:T(8,128)(2,1)} fusion(bf16[1,768,2048]{2,1,0:T(8,128)(2,1)S(1)} %copy-done, bf16[256,2048]{1,0:T(8,128)(2,1)} %reshape_reshape.6, bf16[1,2048,768]{2,1,0:T(8,128)(2,1)} %param.28, f32[256,768]{1,0:T(8,128)} %fusion.15), kind=kOutput, calls=%fused_computation.21 | convolution fusion | flops 1612316672 | bytes 9175040 | tf_op jit(solution)/shard_map/dot_general | solution.py:188
  222.2 2.6 reshape_transpose_transpose_reshape_reshape_reshape.3
  224.8 9.5 %all-to-all-start.2 = ((bf16[128,1,1,2,2048]{4,3,2,1,0:T(2,128)(2,1)}), bf16[128,1,1,2,2048]{4,3,2,1,0:T(2,128)(2,1)}, u32[]{:S(2)}, u32[]{:S(2)}) async-start(bf16[128,1,1,2,2048]{4,3,2,1,0:T(2,128)(2,1)} %bitcast.102), calls=%async_computation.2 | async-start | bytes 2097152 | tf_op jit(solution)/shard_map/all_to_all | solution.py:49
  235.3 28.2 %all-to-all-done.2 = bf16[128,1,1,2,2048]{4,3,2,1,0:T(2,128)(2,1)} async-done(((bf16[128,1,1,2,2048]{4,3,2,1,0:T(2,128)(2,1)}), bf16[128,1,1,2,2048]{4,3,2,1,0:T(2,128)(2,1)}, u32[]{:S(2)}, u32[]{:S(2)}) %all-to-all-start.2) | async-done | bytes 1048608 | tf_op jit(solution)/shard_map/all_to_all | solution.py:49
  263.5 2.3 reshape_reshape.7
  265.7 4.2 %gather_fusion.1 = bf16[192,2048]{1,0:T(8,128)(2,1)} fusion(bf16[256,2048]{1,0:T(8,128)(2,1)} %reshape_reshape.7, s32[1024]{0:T(1024)S(1)} %pad_clamp_fusion), kind=kCustom, calls=%fused_computation.1 | custom fusion | bytes 1573632 | tf_op jit(solution)/shard_map/gather | solution.py:196
  269.9 2.9 %reshape.328 = f32[96,2,2048]{2,1,0:T(2,128)} reshape(bf16[192,2048]{1,0:T(8,128)(2,1)} %gather_fusion.1) | data formatting | bytes 2359296 | tf_op jit(solution)/shard_map/convert_element_type | solution.py:198
  272.9 3.7 %multiply_reduce_fusion = f32[96,2048]{1,0:T(8,128)S(1)} fusion(f32[96,2,2048]{2,1,0:T(2,128)} %reshape.328, f32[96,2]{1,0:T(8,128)S(1)} %copy.90), kind=kLoop, calls=%fused_computation.30 | loop fusion | flops 589824 | bytes 2360064 | tf_op jit(solution)/shard_map/reduce_sum | solution.py:197
  (75 shorter events, 19.9 us)
Async XLA Ops:
  6.5 210.1 %copy-start = (bf16[1,768,2048]{2,1,0:T(8,128)(2,1)S(1)}, bf16[1,768,2048]{2,1,0:T(8,128)(2,1)}, u32[]{:S(2)}) copy-start(bf16[1,768,2048]{2,1,0:T(8,128)(2,1)} %param.29) | copy-start | bytes 9437188
  6.6 4.6 %copy-start.10 = (bf16[512,128]{1,0:T(8,128)(2,1)S(1)}, bf16[512,128]{1,0:T(8,128)(2,1)}, u32[]{:S(2)}) copy-start(bf16[512,128]{1,0:T(8,128)(2,1)} %param.21) | copy-start | bytes 393220
  6.6 89.0 %all-gather.3.cloned.1.call-start = ((), (), s32[]{:S(2)}) async-start(), calls=%async_computation.3 | async-start | bytes 10027008 | tf_op jit(solution)/shard_map/all_gather | solution.py:26
  7.8 3.7 %copy-start.11 = (bf16[512,128]{1,0:T(8,128)(2,1)S(1)}, bf16[512,128]{1,0:T(8,128)(2,1)}, u32[]{:S(2)}) copy-start(bf16[512,128]{1,0:T(8,128)(2,1)} %param.20) | copy-start | bytes 393220
  11.6 4.4 %copy-start.7 = (s32[24,4,2]{0,2,1:T(2,128)S(1)}, s32[24,4,2]{0,2,1:T(2,128)}, u32[]{:S(2)}) copy-start(s32[24,4,2]{0,2,1:T(2,128)} %param.26) | copy-start | bytes 2308
  12.4 0.6 copy-start.2
  12.4 0.7 copy-start.3
  14.1 141.3 %all-gather.5.cloned.1.call-start = ((), (), s32[]{:S(2)}) async-start(), calls=%async_computation.4 | async-start | bytes 4718592 | tf_op jit(solution)/shard_map/all_gather | solution.py:153
  95.6 3.3 %copy-start.4 = (bf16[192,4,32]{2,0,1:T(8,128)(2,1)S(1)}, bf16[192,4,32]{2,0,1:T(8,128)(2,1)}, u32[]{:S(2)}) copy-start(bf16[192,4,32]{2,0,1:T(8,128)(2,1)} %get-tuple-element.5) | copy-start | bytes 147460
  95.6 3.3 %copy-start.5 = (bf16[192,4,32]{2,0,1:T(8,128)(2,1)S(1)}, bf16[192,4,32]{2,0,1:T(8,128)(2,1)}, u32[]{:S(2)}) copy-start(bf16[192,4,32]{2,0,1:T(8,128)(2,1)} %get-tuple-element.6) | copy-start | bytes 147460
  108.2 19.3 %all-to-all-start = ((bf16[192,4,128]{2,1,0:T(4,128)(2,1)}), bf16[192,4,128]{2,1,0:T(4,128)(2,1)S(1)}, u32[]{:S(2)}, u32[]{:S(2)}) async-start(bf16[192,4,128]{2,1,0:T(4,128)(2,1)} %copy.80), calls=%async_computation | async-start | bytes 393216 | tf_op jit(solution)/shard_map/all_to_all | solution.py:148
  127.5 32.1 %copy-start.8 = (f32[2048]{0:T(1024)S(1)}, f32[2048]{0:T(1024)}, u32[]{:S(2)}) copy-start(f32[2048]{0:T(1024)} %param.23) | copy-start | bytes 24580
  158.7 0.9 copy-start.1
  222.2 12.1 %copy-start.6 = (f32[24,4,2]{0,2,1:T(2,128)S(1)}, f32[24,4,2]{0,2,1:T(2,128)}, u32[]{:S(2)}) copy-start(f32[24,4,2]{0,2,1:T(2,128)} %param.25) | copy-start | bytes 2308
  222.2 12.7 %copy-start.9 = (f32[24,4]{0,1:T(4,128)S(1)}, f32[24,4]{0,1:T(4,128)}, u32[]{:S(2)}) copy-start(f32[24,4]{0,1:T(4,128)} %param.24) | copy-start | bytes 1156
  224.8 38.7 %all-to-all-start.2 = ((bf16[128,1,1,2,2048]{4,3,2,1,0:T(2,128)(2,1)}), bf16[128,1,1,2,2048]{4,3,2,1,0:T(2,128)(2,1)}, u32[]{:S(2)}, u32[]{:S(2)}) async-start(bf16[128,1,1,2,2048]{4,3,2,1,0:T(2,128)(2,1)} %bitcast.102), calls=%async_computation.2 | async-start | bytes 2097152 | tf_op jit(solution)/shard_map/all_to_all | solution.py:49
Sparse Core Ops, SparseCore 0:
  14.2 81.3 all-gather.2
  97.4 57.9 all-gather.4
where the time goes:
time: 286 us
  waiting for transfers between devices  140 us (49%)
  blocking collectives  42.9 us (15%)
  local copies, waits for them, and re-layouts  34.9 us (12%)
  matrix products  24.3 us (8%)
  starting transfers between devices  16 us (6%)
  between operations  13.8 us (5%)
  other arithmetic  13.4 us (5%)
    all_gather x1, waiting for transfers between devices, side_by_side(): out = lax.all_gather(both, axis, axis=dim, tiled=True)  74 us
    all_to_all x1, blocking collectives, joined_exchange(): lax.all_to_all(pieces, axis, split_axis=0, concat_axis=0, tiled=True)  42.9 us
    all_to_all x1, waiting for transfers between devices, joined_exchange(): lax.all_to_all(pieces, axis, split_axis=0, concat_axis=0, tiled=True)  28.2 us
    all_gather x1, waiting for transfers between devices, shards(): lax.all_gather(out_weight, 'tp', axis=0, tiled=True)  27.8 us
    all_to_all x1, waiting for transfers between devices, shards(): lax.all_to_all(attended, 'tp', split_axis=0, concat_axis=2, tiled=True)  9.53 us
    all_to_all x1, starting transfers between devices, joined_exchange(): lax.all_to_all(pieces, axis, split_axis=0, concat_axis=0, tiled=True)  9.5 us
    all_to_all x1, starting transfers between devices, shards(): lax.all_to_all(attended, 'tp', split_axis=0, concat_axis=2, tiled=True)  6.42 us
  transfers between devices with their start and end apart: 4, of which 4 were waited for; matrix products, arithmetic and copies ran while one was open for 8% of the time, Pallas kernels for 0%

commit v1 on v0

--- a/solution.py
+++ b/solution.py
@@ -1,8 +1,11 @@
+import functools
 import math
 
 import jax
 import jax.numpy as jnp
 from jax import lax
+from jax.experimental import pallas as pl
+from jax.experimental.pallas import tpu as pltpu
 from jax.sharding import PartitionSpec as P
 
 D = 2048
@@ -11,6 +14,9 @@
 QK = 192
 TOPK = 2
 SEQS = 4
+CAP = 2
+LANES = 128
+MESH = pl.DeviceIdType.MESH
 
 
 epsilon = 1e-06
@@ -26,29 +32,6 @@
     out = lax.all_gather(both, axis, axis=dim, tiled=True)
     pieces = jnp.split(out, [sum(widths[:k]) for k in range(1, len(widths))], axis=along)
     return tuple((b.reshape(*out.shape[:along], *a.shape[along:]) for a, b in zip(arrays, pieces)))
-
-
-def in_blocks(shard, dim, peers):
-    dims = shard.shape
-    pieces = shard.reshape(*dims[:dim], peers, dims[dim] // peers, *dims[dim + 1 :])
-    return jnp.moveaxis(pieces, dim, 0)
-
-
-def laid_out(pieces, dim):
-    pieces = jnp.moveaxis(pieces, 0, dim)
-    dims = pieces.shape
-    return pieces.reshape(*dims[:dim], dims[dim] * dims[dim + 1], *dims[dim + 2 :])
-
-
-def joined_exchange(shard, axis, axes, splits, concats):
-    sizes = [lax.axis_size(a) for a in axes]
-    pieces = in_blocks(shard, splits[0], sizes[0])
-    pieces = jnp.moveaxis(in_blocks(pieces, splits[1] + 1, sizes[1]), 0, 1)
-    inside = pieces.shape[2:]
-    pieces = pieces.reshape(-1, *inside)
-    pieces = lax.all_to_all(pieces, axis, split_axis=0, concat_axis=0, tiled=True)
-    pieces = laid_out(pieces.reshape(*sizes, *inside), concats[0] + 1)
-    return laid_out(pieces, concats[1])
 
 
 def rotate(values, positions):
@@ -105,6 +88,164 @@
         preferred_element_type=jnp.float32,
     )
     return (highest, totals, accumulated)
+
+
+def moe_kernel(sp_n, tp_n, normed_ref, stream_ref, routes_ref, mix_ref, wg_hbm, wu_hbm, wd_hbm, out_ref,
+               wg, wu, wd, stage, outgoing, arrived, leaving, returned, rows_in, w_sems, send_sem, recv_sem, back_send, back_recv):
+    peers = sp_n * tp_n
+    rows, width = normed_ref.shape
+    chunks = width // LANES
+    sp, tp = lax.axis_index("sp"), lax.axis_index("tp")
+    me = sp * tp_n + tp
+    barrier = pltpu.get_barrier_semaphore()
+
+    def peer(i):
+        other = lax.rem(me + i, peers)
+        return other, {"sp": other // tp_n, "tp": lax.rem(other, tp_n)}
+
+    def greet(i, _):
+        pl.semaphore_signal(barrier, inc=1, device_id=peer(i)[1], device_id_type=MESH)
+        return 0
+
+    lax.fori_loop(1, peers, greet, 0)
+    loads = [
+        pltpu.make_async_copy(src, dst, w_sems.at[k])
+        for k, (src, dst) in enumerate(((wg_hbm, wg), (wu_hbm, wu), (wd_hbm, wd)))
+    ]
+    for load in loads:
+        load.start()
+
+    experts = lax.broadcasted_iota(jnp.int32, (rows, peers), 1)
+    picks = [(routes_ref[:, k : k + 1] == experts).astype(jnp.float32) for k in range(TOPK)]
+    both = (picks[0] + picks[1]).astype(jnp.bfloat16)
+    earlier = (
+        lax.broadcasted_iota(jnp.int32, (rows, rows), 0) > lax.broadcasted_iota(jnp.int32, (rows, rows), 1)
+    ).astype(jnp.float32).astype(jnp.bfloat16)
+    before = jnp.dot(earlier, both, preferred_element_type=jnp.float32)
+    chosen = []
+    for pick in picks:
+        slot = jnp.sum(pick * before, axis=1, keepdims=True)
+        chosen.append(jnp.concatenate([pick * (1.0 - slot), pick * slot], axis=1))
+    taken = (chosen[0] + chosen[1]).astype(jnp.bfloat16)
+    chosen = [c.astype(jnp.bfloat16) for c in chosen]
+
+    for j in range(chunks // 2):
+        part = lax.dot_general(
+            taken, normed_ref[:, 2 * j * LANES : (2 * j + 2) * LANES], (((0,), (0,)), ((), ())),
+            preferred_element_type=jnp.float32,
+        )
+        for c in range(CAP):
+            for h in range(2):
+                stage[pl.ds(c * chunks + 2 * j + h, peers, stride=CAP * chunks), :] = part[
+                    c * peers : (c + 1) * peers, h * LANES : (h + 1) * LANES
+                ]
+    step = min(8, peers)
+    span = CAP * chunks
+
+    def pack(dst):
+        def body(i, _):
+            rows_at = pl.ds(pl.multiple_of(i * step * span, step * span), step * span)
+            dst[pl.ds(i * step, step)] = stage[rows_at, :].astype(jnp.bfloat16).reshape(step, span, LANES)
+            return 0
+
+        lax.fori_loop(0, peers // step, body, 0)
+
+    def unpack(src):
+        def body(i, _):
+            rows_at = pl.ds(pl.multiple_of(i * step * span, step * span), step * span)
+            stage[rows_at, :] = src[pl.ds(i * step, step)].astype(jnp.float32).reshape(step * span, LANES)
+            return 0
+
+        lax.fori_loop(0, peers // step, body, 0)
+
+    def exchange(src, dst, sent, got):
+        def body(i, _):
+            other, where = peer(i)
+            pltpu.make_async_remote_copy(
+                src_ref=src.at[other], dst_ref=dst.at[me], send_sem=sent, recv_sem=got, device_id=where,
+                device_id_type=MESH,
+            ).start()
+            return 0
+
+        lax.fori_loop(1, peers, body, 0)
+        dst[me] = src[me]
+
+    def settle(buffer, sem):
+        many = buffer.at[pl.ds(0, peers - 1)]
+        pltpu.make_async_copy(many, many, sem).wait()
+
+    pack(outgoing)
+    pl.semaphore_wait(barrier, peers - 1)
+    exchange(outgoing, arrived, send_sem, recv_sem)
+    for load in loads:
+        load.wait()
+    settle(arrived, recv_sem)
+
+    unpack(arrived)
+    total = peers * CAP
+    for l in range(chunks):
+        rows_in[:, l * LANES : (l + 1) * LANES] = stage[pl.ds(l, total, stride=chunks), :].astype(jnp.bfloat16)
+    tile = 256
+    hidden = []
+    for j in range(wg.shape[1] // tile):
+        cols = slice(j * tile, (j + 1) * tile)
+        gate = jnp.dot(rows_in[...], wg[:, cols], preferred_element_type=jnp.float32)
+        up = jnp.dot(rows_in[...], wu[:, cols], preferred_element_type=jnp.float32)
+        hidden.append((gate / (1.0 + jnp.exp(-gate)) * up).astype(jnp.bfloat16))
+    hidden = jnp.concatenate(hidden, axis=1)
+    for j in range(chunks // 2):
+        part = jnp.dot(hidden, wd[:, 2 * j * LANES : (2 * j + 2) * LANES], preferred_element_type=jnp.float32)
+        for h in range(2):
+            stage[pl.ds(2 * j + h, total, stride=chunks), :] = part[:, h * LANES : (h + 1) * LANES]
+    pack(leaving)
+    exchange(leaving, returned, back_send, back_recv)
+    settle(outgoing, send_sem)
+    settle(returned, back_recv)
+
+    unpack(returned)
+    for j in range(chunks // 2):
+        block = jnp.concatenate(
+            [
+                jnp.concatenate(
+                    [stage[pl.ds(c * chunks + 2 * j + h, peers, stride=span), :] for c in range(CAP)], axis=0
+                )
+                for h in range(2)
+            ],
+            axis=1,
+        ).astype(jnp.bfloat16)
+        cols = slice(2 * j * LANES, (2 * j + 2) * LANES)
+        added = mix_ref[:, 0:1] * jnp.dot(chosen[0], block, preferred_element_type=jnp.float32) + mix_ref[
+            :, 1:2
+        ] * jnp.dot(chosen[1], block, preferred_element_type=jnp.float32)
+        out_ref[:, cols] = (stream_ref[:, cols].astype(jnp.float32) + added).astype(jnp.bfloat16)
+    settle(leaving, back_send)
+
+
+def routed_experts(sp_n, tp_n, normed, stream, routes, mixing, w_gate, w_up, w_down):
+    rows, width = normed.shape
+    peers = sp_n * tp_n
+    span = CAP * width // LANES
+    vmem = pl.BlockSpec(memory_space=pltpu.VMEM)
+    hbm = pl.BlockSpec(memory_space=pl.ANY)
+    blocks = pltpu.VMEM((peers, span, LANES), jnp.bfloat16)
+    dma = pltpu.SemaphoreType.DMA
+    return pl.pallas_call(
+        functools.partial(moe_kernel, sp_n, tp_n),
+        out_shape=jax.ShapeDtypeStruct((rows, width), jnp.bfloat16),
+        in_specs=[vmem] * 4 + [hbm] * 3,
+        out_specs=vmem,
+        scratch_shapes=[
+            pltpu.VMEM(w_gate.shape, jnp.bfloat16),
+            pltpu.VMEM(w_up.shape, jnp.bfloat16),
+            pltpu.VMEM(w_down.shape, jnp.bfloat16),
+            pltpu.VMEM((peers * span, LANES), jnp.float32),
+            blocks, blocks, blocks, blocks,
+            pltpu.VMEM((peers * CAP, width), jnp.bfloat16),
+            dma((3,)), dma, dma, dma, dma,
+        ],
+        compiler_params=pltpu.CompilerParams(collective_id=1, has_side_effects=True),
+        name="routed_experts",
+    )(normed, stream, routes, mixing, w_gate, w_up, w_down)
 
 
 def shards(
@@ -158,46 +299,18 @@
     mixing = jax.nn.softmax(pair_logits.reshape(row_count, TOPK), axis=-1) * group_prob.reshape(
         row_count, 1
     )
-    experts_total = lax.axis_size("sp") * lax.axis_size("tp")
-    capacity = max(2, 3 * row_count * TOPK // (2 * experts_total))
-    pick_count = row_count * TOPK
-    chosen = routes.reshape(pick_count)
-    one_hot = (chosen[:, None] == jnp.arange(experts_total, dtype=jnp.int32)[None, :]).astype(
-        jnp.bfloat16
-    )
-    earlier = (jnp.arange(pick_count)[:, None] > jnp.arange(pick_count)[None, :]).astype(
-        jnp.bfloat16
-    )
-    before = jnp.dot(earlier, one_hot, preferred_element_type=jnp.float32)
-    slot_index = jnp.sum(before * one_hot.astype(jnp.float32), axis=-1).astype(jnp.int32)
-    target = chosen * capacity + slot_index
-    source_row = (
-        jnp.full((experts_total * capacity,), row_count, jnp.int32)
-        .at[target]
-        .set(jnp.arange(pick_count, dtype=jnp.int32) // TOPK)
-    )
-    padded = jnp.concatenate([normed, jnp.zeros((1, D), jnp.bfloat16)], axis=0)
-    outgoing = padded[source_row].reshape(experts_total, capacity, D)
-    sectioned = outgoing.reshape(lax.axis_size("sp"), lax.axis_size("tp"), capacity, D)
-    arrived = joined_exchange(sectioned, ("sp", "tp"), ("sp", "tp"), (0, 1), (0, 1))
-    flat_rows = arrived.reshape(-1, D)
-    gate_pre = jnp.dot(flat_rows, w_gate[0], preferred_element_type=jnp.float32)
-    upward = jnp.dot(flat_rows, w_up[0], preferred_element_type=jnp.float32)
-    hidden = (jax.nn.silu(gate_pre) * upward).astype(jnp.bfloat16)
-    returned = joined_exchange(
-        jnp.dot(hidden, w_down[0], preferred_element_type=jnp.float32)
-        .astype(jnp.bfloat16)
-        .reshape(arrived.shape),
-        ("sp", "tp"),
-        ("sp", "tp"),
-        (0, 1),
-        (0, 1),
-    )
-    results = returned.reshape(experts_total * capacity, D)[target].reshape(row_count, TOPK, D)
-    combined = stream.astype(jnp.float32) + jnp.sum(
-        results.astype(jnp.float32) * mixing[..., None], axis=1
-    )
-    return combined.astype(jnp.bfloat16).reshape(residual.shape)
+    combined = routed_experts(
+        lax.axis_size("sp"),
+        lax.axis_size("tp"),
+        normed,
+        stream,
+        routes.reshape(row_count, TOPK),
+        mixing,
+        w_gate[0],
+        w_up[0],
+        w_down[0],
+    )
+    return combined.reshape(residual.shape)
 
 
 def solution(mesh):

time: 286 us -> 275 us (0.962)
  Pallas kernels: 0 us -> 107 us
  blocking collectives: 42.9 us -> 0 us
  local copies, waits for them, and re-layouts: 34.9 us -> 5.44 us
  waiting for transfers between devices: 140 us -> 120 us
  matrix products: 24.3 us -> 14.2 us
  starting transfers between devices: 16 us -> 6.49 us
  other arithmetic: 13.4 us -> 8.28 us
    pallas_call x0 -> x1, Pallas kernels: none -> 107 us  [routed_experts(): pl.pallas_call(functools.partial(moe_kernel, sp_n, tp_n), out_shape=jax.S...]
    all_to_all x1 -> x0, blocking collectives: 42.9 us -> none  [joined_exchange(): lax.all_to_all(pieces, axis, split_axis=0, concat_axis=0, tiled=True)]
    all_to_all x1 -> x0, waiting for transfers between devices: 28.2 us -> none  [joined_exchange(): lax.all_to_all(pieces, axis, split_axis=0, concat_axis=0, tiled=True)]
    dot_general x3 -> x0, matrix products: 9.99 us -> none  [the longest x1 5.55 us: shards(): jnp.dot(hidden, w_down[0], preferred_element_type=jnp.float32)]
    another operation x4 -> x0, local copies, waits for them, and re-layouts: 9.6 us -> none  [the longest x2 5.09 us: joined_exchange(): pieces = pieces.reshape(-1, *inside)]
    all_to_all x1 -> x0, starting transfers between devices: 9.5 us -> none  [joined_exchange(): lax.all_to_all(pieces, axis, split_axis=0, concat_axis=0, tiled=True)]
    gather x2 -> x0, local copies, waits for them, and re-layouts: 8.57 us -> none  [the longest x1 4.4 us: shards(): outgoing = padded[source_row].reshape(experts_total, capacity, D)]
    all_gather x1, waiting for transfers between devices: 74 us -> 80.4 us  [side_by_side(): out = lax.all_gather(both, axis, axis=dim, tiled=True)]
  transfers between devices with their start and end apart: 4 -> 3, of which waited for: 4 -> 3; matrix products, arithmetic and copies ran while one was open for 8% -> 6% of each run, Pallas kernels for 0% -> 0%
where the time goes in v1:
time: 275 us; the launch traced here: 274 us
  waiting for transfers between devices  120 us (44%)
  Pallas kernels  107 us (39%)
  matrix products  14.2 us (5%)
  between operations  13.7 us (5%)
  other arithmetic  8.28 us (3%)
  starting transfers between devices  6.49 us (2%)
  local copies, waits for them, and re-layouts  5.44 us (2%)
    pallas_call x1, Pallas kernels, routed_experts(): pl.pallas_call(functools.partial(moe_kernel, sp_n, tp_n), out_shape=jax.S...  107 us
    all_gather x1, waiting for transfers between devices, side_by_side(): out = lax.all_gather(both, axis, axis=dim, tiled=True)  80.4 us
    all_gather x1, waiting for transfers between devices, shards(): lax.all_gather(out_weight, 'tp', axis=0, tiled=True)  27.8 us
    all_to_all x1, waiting for transfers between devices, shards(): lax.all_to_all(attended, 'tp', split_axis=0, concat_axis=2, tiled=True)  10.6 us
    all_to_all x1, starting transfers between devices, shards(): lax.all_to_all(attended, 'tp', split_axis=0, concat_axis=2, tiled=True)  6.42 us
  transfers between devices with their start and end apart: 3, of which 3 were waited for; matrix products, arithmetic and copies ran while one was open for 6% of the time, Pallas kernels for 0%

profile of v1, /device:TPU:513, one launch (start us, length us, event | category | flops | bytes accessed | tf_op | source)
XLA Modules:
  0.0 274.3 jit_solution(7039975783180830131)
XLA Ops:
  6.6 1.1 copy.69
  7.7 1.6 fusion.12
  9.4 1.7 fusion.14
  11.1 0.4 convolution_convert_fusion
  11.5 0.4 convolution_convert_fusion.1
  11.9 0.4 multiply_cosine_fusion
  12.3 0.2 subtract_convert_fusion.1
  12.5 1.0 pad_maximum_fusion
  13.6 0.7 all-gather.5.cloned.1.call-update
  14.6 80.4 %all-gather.3.cloned.1.call-done = bf16[3072,4,320]{2,0,1:T(8,128)(2,1)} async-done(((bf16[192,4,320]{2,0,1:T(8,128)(2,1)}), bf16[3072,4,320]{2,0,1:T(8,128)(2,1)}) %all-gather.3.cloned.1.call-update) | async-done | bytes 7864336 | tf_op jit(solution)/shard_map/all_gather | solution.py:32
  95.0 3.3 %fusion.9 = f32[4,3072,192]{1,2,0:T(8,128)S(1)} fusion(bf16[3072,4,320]{2,0,1:T(8,128)(2,1)} %all-gather.3.cloned.1.call-done, bf16[192,4,1,192]{3,0,1,2:T(8,128)(2,1)S(1)} %bitcast.68), kind=kOutput, calls=%fused_computation.10 | convolution fusion | flops 603979776 | bytes 12779520 | tf_op jit(solution)/shard_map/qshd,kshd->qshk/dot_general | solution.py:76
  98.3 3.3 %fusion.50 = (f32[192,4]{0,1:T(4,128)S(1)}, f32[192,4,1,3072]{3,0,1,2:T(8,128)S(1)}) fusion(bf16[192,4,32]{2,0,1:T(8,128)(2,1)S(1)} %get-tuple-element.6, bf16[192,4,32]{2,0,1:T(8,128)(2,1)S(1)} %get-tuple-element.5, bf16[3072,4,320]{2,0,1:T(8,128)(2,1)} %all-gather.3.cloned.1.call-done, f32[4,3072,192]{1,2,0:T(8,128)S(1)} %fusion.9), kind=kOutput, calls=%fused_computation.59 | convolution fusion | flops 309263616 | bytes 22121472 | tf_op jit(solution)/shard_map/qshd,ksd->qshk/dot_general | solution.py:77
  101.6 1.4 fusion.1
  103.1 3.7 %fusion.30 = bf16[192,4,128]{2,0,1:T(8,128)(2,1)S(1)} fusion(bf16[3072,4,320]{2,0,1:T(8,128)(2,1)} %all-gather.3.cloned.1.call-done, f32[192,4,1,3072]{3,0,1,2:T(8,128)S(1)} %get-tuple-element.12, f32[192,4]{0,1:T(4,128)S(1)} %broadcast_maximum_fusion, f32[192,4]{0,1:T(4,128)S(1)} %fusion.1), kind=kOutput, calls=%fused_computation.24 | convolution fusion | flops 608894976 | bytes 12785664 | tf_op jit(solution)/shard_map/qshk,kshd->qshd/dot_general | solution.py:84
  106.8 0.8 copy.73
  107.6 6.4 %all-to-all-start = ((bf16[192,4,128]{2,1,0:T(4,128)(2,1)}), bf16[192,4,128]{2,1,0:T(4,128)(2,1)S(1)}, u32[]{:S(2)}, u32[]{:S(2)}) async-start(bf16[192,4,128]{2,1,0:T(4,128)(2,1)} %copy.73), calls=%async_computation | async-start | bytes 393216 | tf_op jit(solution)/shard_map/all_to_all | solution.py:289
  114.9 0.7 copy.75
  115.6 0.7 divide_multiply_fusion.mix_ref
  116.3 10.6 %all-to-all-done = bf16[192,4,128]{2,1,0:T(4,128)(2,1)S(1)} async-done(((bf16[192,4,128]{2,1,0:T(4,128)(2,1)}), bf16[192,4,128]{2,1,0:T(4,128)(2,1)S(1)}, u32[]{:S(2)}, u32[]{:S(2)}) %all-to-all-start) | async-done | bytes 196640 | tf_op jit(solution)/shard_map/all_to_all | solution.py:289
  127.0 27.8 %all-gather.5.cloned.1.call-done = bf16[1024,2048]{1,0:T(8,128)(2,1)} async-done(((bf16[128,2048]{1,0:T(8,128)(2,1)}), bf16[1024,2048]{1,0:T(8,128)(2,1)}) %all-gather.5.cloned.1.call-update) | async-done | bytes 4194320 | tf_op jit(solution)/shard_map/all_gather | solution.py:294
  154.8 3.1 %fusion.35 = (f32[96]{0:T(128)S(1)}, bf16[96,2048]{1,0:T(8,128)(2,1)S(1)}) fusion(f32[96,2048]{1,0:T(8,128)S(1)} %reshape.219, bf16[1024,2048]{1,0:T(8,128)(2,1)} %all-gather.5.cloned.1.call-done, bf16[12,8,8,128]{3,2,1,0:T(8,128)(2,1)S(1)} %bitcast.69), kind=kOutput, calls=%fused_computation.27 | convolution fusion | flops 403636128 | bytes 5570944 | tf_op jit(solution)/shard_map/dot_general | solution.py:292
  157.9 0.9 fusion.37.normed_ref
  158.9 106.7 %routed_experts.1 = bf16[96,2048]{1,0:T(8,128)(2,1)} custom-call(bf16[96,2048]{1,0:T(8,128)(2,1)} %fusion.37.normed_ref, bf16[96,2048]{1,0:T(8,128)(2,1)} %copy-done.1, s32[96,2]{1,0:T(8,128)} %bitcast.71, f32[96,2]{1,0:T(8,128)} %divide_multiply_fusion.mix_ref, bf16[2048,768]{1,0:T(8,128)(2,1)} %bitcast.64, bf16[2048,768]{1,0:T(8,128)(2,1)} %bitcast.65, ...), custom_call_target="tpu_custom_call" | custom-call | tf_op jit(solution)/shard_map/routed_experts/pallas_call | solution.py:232
  265.6 1.9 reshape.218
  (41 shorter events, 1.4 us)
Async XLA Ops:
  6.5 4.5 %copy-start = (bf16[512,128]{1,0:T(8,128)(2,1)S(1)}, bf16[512,128]{1,0:T(8,128)(2,1)}, u32[]{:S(2)}) copy-start(bf16[512,128]{1,0:T(8,128)(2,1)} %param.21) | copy-start | bytes 393220
  6.6 4.9 %copy-start.8 = (bf16[512,128]{1,0:T(8,128)(2,1)S(1)}, bf16[512,128]{1,0:T(8,128)(2,1)}, u32[]{:S(2)}) copy-start(bf16[512,128]{1,0:T(8,128)(2,1)} %param.20) | copy-start | bytes 393220
  6.6 88.4 %all-gather.3.cloned.1.call-start = ((), (), s32[]{:S(2)}) async-start(), calls=%async_computation.1 | async-start | bytes 10027008 | tf_op jit(solution)/shard_map/all_gather | solution.py:32
  9.4 5.0 %copy-start.2 = (bf16[192,4,192]{2,1,0:T(4,128)(2,1)S(1)}, bf16[192,4,192]{2,1,0:T(4,128)(2,1)}, u32[]{:S(2)}) copy-start(bf16[192,4,192]{2,1,0:T(4,128)(2,1)} %param.16) | copy-start | bytes 884740
  13.5 141.3 %all-gather.5.cloned.1.call-start = ((), (), s32[]{:S(2)}) async-start(), calls=%async_computation.2 | async-start | bytes 4718592 | tf_op jit(solution)/shard_map/all_gather | solution.py:294
  103.0 11.0 %copy-start.3 = (bf16[24,4,2048]{2,1,0:T(4,128)(2,1)S(1)}, bf16[24,4,2048]{2,1,0:T(4,128)(2,1)}, u32[]{:S(2)}) copy-start(bf16[24,4,2048]{2,1,0:T(4,128)(2,1)} %param.15) | copy-start | bytes 1179652
  103.0 11.1 %copy-start.4 = (f32[24,4,2]{0,2,1:T(2,128)S(1)}, f32[24,4,2]{0,2,1:T(2,128)}, u32[]{:S(2)}) copy-start(f32[24,4,2]{0,2,1:T(2,128)} %param.25) | copy-start | bytes 2308
  103.1 11.6 %copy-start.7 = (f32[24,4]{0,1:T(4,128)S(1)}, f32[24,4]{0,1:T(4,128)}, u32[]{:S(2)}) copy-start(f32[24,4]{0,1:T(4,128)} %param.24) | copy-start | bytes 1156
  103.1 11.8 %copy-start.6 = (s32[24,4,2]{0,2,1:T(2,128)S(1)}, s32[24,4,2]{0,2,1:T(2,128)}, u32[]{:S(2)}) copy-start(s32[24,4,2]{0,2,1:T(2,128)} %param.26) | copy-start | bytes 2308
  106.8 51.2 %copy-start.5 = (f32[2048]{0:T(1024)S(1)}, f32[2048]{0:T(1024)}, u32[]{:S(2)}) copy-start(f32[2048]{0:T(1024)} %param.23) | copy-start | bytes 24580
  107.6 19.3 %all-to-all-start = ((bf16[192,4,128]{2,1,0:T(4,128)(2,1)}), bf16[192,4,128]{2,1,0:T(4,128)(2,1)S(1)}, u32[]{:S(2)}, u32[]{:S(2)}) async-start(bf16[192,4,128]{2,1,0:T(4,128)(2,1)} %copy.73), calls=%async_computation | async-start | bytes 393216 | tf_op jit(solution)/shard_map/all_to_all | solution.py:289
  157.9 0.9 copy-start.1
Sparse Core Ops, SparseCore 0:
  13.6 81.3 all-gather.2
  96.8 57.9 all-gather.4

commit v2 on v1

--- a/solution.py
+++ b/solution.py
@@ -10,10 +10,8 @@
 
 D = 2048
 NOPE = 128
-VDIM = 128
 QK = 192
 TOPK = 2
-SEQS = 4
 CAP = 2
 LANES = 128
 MESH = pl.DeviceIdType.MESH
@@ -21,24 +19,12 @@
 
 epsilon = 1e-06
 rotary_base = 10000.0
-lowest = -1e30
-
-
-def side_by_side(arrays, axis, dim, along):
-    widths = [math.prod(a.shape[along:]) for a in arrays]
-    both = jnp.concatenate(
-        [a.reshape(*a.shape[:along], w) for a, w in zip(arrays, widths)], axis=along
-    )
-    out = lax.all_gather(both, axis, axis=dim, tiled=True)
-    pieces = jnp.split(out, [sum(widths[:k]) for k in range(1, len(widths))], axis=along)
-    return tuple((b.reshape(*out.shape[:along], *a.shape[along:]) for a, b in zip(arrays, pieces)))
-
-
-def rotate(values, positions):
+
+
+def rotate_by(values, positions):
     halfway = values.shape[-1] // 2
     inverse = rotary_base ** (-jnp.arange(halfway, dtype=jnp.float32) / halfway)
     angles = positions.astype(jnp.float32)[:, None] * inverse[None, :]
-    angles = angles.reshape((angles.shape[0],) + (1,) * (values.ndim - 2) + (halfway,))
     cosine_values = jnp.cos(angles)
     sine_values = jnp.sin(angles)
     first_half = values[..., :halfway]
@@ -60,34 +46,251 @@
     )
 
 
-def expand(latent_rows, latent_gain, key_up, value_up):
-    normed = rms_scale(latent_rows.astype(jnp.float32), latent_gain).astype(jnp.bfloat16)
-    keys_nope = jnp.dot(normed, key_up, preferred_element_type=jnp.float32).astype(jnp.bfloat16)
+def attention_kernel(sp_n, tp_n, seqs, q_ref, kv_ref, ow_ref, res_ref, gain_ref, stream_ref, normed_ref,
+                     kv_all, q_all, ow_all, att, heads_y, heads_in, run_max, run_sum, acc,
+                     kv_sem, kv_fwd, kv_sib, q_sem, ow_sem, ow_sib, y_sem, x_sem, kv_sent, q_sent, ow_sent, ow_half, ow_sib_sent, y_sent, x_sent):
+    chips = sp_n // 2
+    side = chips // 2
+    half_ring = tp_n // 2
+    sp, tp = lax.axis_index("sp"), lax.axis_index("tp")
+    chip, core = sp // 2, lax.rem(sp, 2)
+    own_seq, own_g = chip // 2, lax.rem(chip, 2)
+    positions = q_ref.shape[1]
+    half = positions // 2
+    part = ow_ref.shape[0] // 2
+
+    def at(chip_id, core_id=None):
+        return {"sp": 2 * chip_id + (core if core_id is None else core_id)}
+
+    homes = []
+    for e in range(1, seqs):
+        seq = lax.rem(own_seq + e, seqs)
+        delta = lax.rem(chip - 2 * seq + chips, chips)
+        g = 1 - lax.rem(delta + chips - 1, chips) // side
+        home = 2 * seq + g
+        k = g * lax.rem(chip - home + chips, chips) + (1 - g) * lax.rem(home - chip + chips, chips)
+        homes.append((seq, g, home, k))
+    sources = [lax.rem(chip + (2 * own_g - 1) * k + chips, chips) for k in range(side)]
+    beside = 2 * own_seq + 1 - own_g
+    right, left = lax.rem(tp + 1, tp_n), lax.rem(tp + tp_n - 1, tp_n)
+
+    def slot(core_id, g, k):
+        return (core_id * 2 + g) * side + k
+
+    def send(src, dst, sent, got, where):
+        pltpu.make_async_remote_copy(
+            src_ref=src, dst_ref=dst, send_sem=sent, recv_sem=got, device_id=where, device_id_type=MESH
+        ).start()
+
+    def landed(buffer, sem):
+        pltpu.make_async_copy(buffer, buffer, sem).wait()
+
+    barrier = pltpu.get_barrier_semaphore()
+    peers = [at(h[2]) for h in homes] + [at(s) for s in sources[1:]] + [at(beside), at(chip, 1 - core)]
+    peers += [{"tp": lax.rem(tp + d, tp_n)} for d in range(1, tp_n)]
+    for where in peers:
+        pl.semaphore_signal(barrier, inc=1, device_id=where, device_id_type=MESH)
+    pl.semaphore_wait(barrier, len(peers))
+
+    own_slot = slot(core, own_g, 0)
+    for seq, g, home, k in homes:
+        send(kv_ref.at[seq], kv_all.at[slot(core, g, k)], kv_sent, kv_sem.at[k], at(home))
+        send(q_ref.at[seq], q_all.at[k], q_sent, q_sem.at[k], at(home))
+
+    def ow_stage(r):
+        for way, to in ((0, right), (1, left)):
+            head = lax.rem(tp + (r - 1 if way else 1 - r) + tp_n, tp_n)
+            if r < half_ring:
+                src = ow_ref.at[pl.ds(core * part, part)] if r == 1 else ow_all.at[head, core]
+                send(src, ow_all.at[head, core], ow_sent, ow_sem.at[way, r - 1], {"tp": to})
+            else:
+                rows = pl.ds(way * (part // 2), part // 2)
+                src = ow_ref.at[pl.ds(core * part + way * (part // 2), part // 2)] if r == 1 else ow_all.at[head, core, rows]
+                send(src, ow_all.at[head, core, rows], ow_half, ow_sem.at[way, r - 1], {"tp": to})
+
+    def ow_arrived(r):
+        for way in range(2):
+            head = lax.rem(tp + (r if way else -r) + tp_n, tp_n)
+            if r < half_ring:
+                landed(ow_all.at[head, core], ow_sem.at[way, r - 1])
+            else:
+                landed(ow_all.at[head, core, pl.ds(way * (part // 2), part // 2)], ow_sem.at[way, r - 1])
+            if r < half_ring or way == 1:
+                send(ow_all.at[head, core], ow_all.at[head, core], ow_sib_sent, ow_sib, at(chip, 1 - core))
+        if r < half_ring:
+            ow_stage(r + 1)
+
+    def pass_on(k, src):
+        place = kv_all.at[slot(core, own_g, k)]
+        send(src, place, kv_sent, kv_fwd.at[k], at(beside))
+        send(src, place, kv_sent, kv_sib.at[own_g, k], at(chip, 1 - core))
+
+    ow_stage(1)
+    pass_on(0, kv_ref.at[own_seq])
+    kv_all[own_slot] = kv_ref[own_seq]
+    q_all[0] = q_ref[own_seq]
+    ow_all[tp] = ow_ref[...].reshape(ow_all.shape[1:])
+
+    lane = lax.broadcasted_iota(jnp.int32, (positions, 2 * LANES), 1)
+    low = lane < LANES + LANES // 2
+    high = (lane < LANES) | (lane >= LANES + LANES // 2)
+    factor = QK ** (-0.5) * math.log2(math.e)
+
+    def attend(base, k, first, last):
+        def rows(start):
+            return kv_all[pl.ds(base, side), start : start + half, :].reshape(side * half, LANES)
+
+        q = q_all[k]
+        turned = rows(4 * half)
+        scores = []
+        for n, mask in ((0, low), (1, high)):
+            keys = jnp.concatenate([rows(n * half), turned], axis=1)
+            scores.append(
+                lax.dot_general(
+                    jnp.where(mask, q, jnp.zeros_like(q)), keys, (((1,), (1,)), ((), ())),
+                    preferred_element_type=jnp.float32,
+                )
+            )
+        top = jnp.maximum(jnp.max(scores[0], axis=1, keepdims=True), jnp.max(scores[1], axis=1, keepdims=True))
+        if not first:
+            old = run_max[k][:, :1]
+            top = jnp.maximum(top, old)
+            shrink = jnp.exp2((old - top) * factor)
+        total, mixed = 0.0, 0.0
+        for n in range(2):
+            weights = jnp.exp2((scores[n] - top) * factor)
+            total = total + jnp.sum(weights, axis=1, keepdims=True)
+            mixed = mixed + jnp.dot(weights.astype(jnp.bfloat16), rows((2 + n) * half), preferred_element_type=jnp.float32)
+        if not first:
+            total = total + shrink * run_sum[k][:, :1]
+            mixed = mixed + shrink * acc[k]
+        if last:
+            att[k] = (mixed / total).reshape(att.shape[1:]).astype(jnp.bfloat16)
+        else:
+            run_max[k] = jnp.broadcast_to(top, run_max.shape[1:])
+            run_sum[k] = jnp.broadcast_to(total, run_sum.shape[1:])
+            acc[k] = mixed
+
+    def attend_all(base, first):
+        def body(k, _):
+            attend(base, k, first, False)
+            return 0
+
+        lax.fori_loop(0, side, body, 0)
+
+    for k in range(1, side):
+        landed(kv_all.at[slot(core, own_g, k)], kv_sem.at[k])
+        pass_on(k, kv_all.at[slot(core, own_g, k)])
+        if k < half_ring:
+            ow_arrived(k)
+    for k in range(1, side):
+        landed(q_all.at[k], q_sem.at[k])
+    attend_all(slot(core, own_g, 0), True)
+    for k in range(side):
+        landed(kv_all.at[slot(1 - core, own_g, k)], kv_sib.at[own_g, k])
+    attend_all(slot(1 - core, own_g, 0), False)
+    for k in range(side):
+        place = kv_all.at[slot(core, 1 - own_g, k)]
+        landed(place, kv_fwd.at[k])
+        send(place, place, kv_sent, kv_sib.at[1 - own_g, k], at(chip, 1 - core))
+    for r in range(min(side, half_ring), half_ring + 1):
+        ow_arrived(r)
+    attend_all(slot(core, 1 - own_g, 0), False)
+    for k in range(side):
+        landed(kv_all.at[slot(1 - core, 1 - own_g, k)], kv_sib.at[1 - own_g, k])
+    for k in list(range(1, side)) + [0]:
+        attend(slot(1 - core, 1 - own_g, 0), k, False, True)
+        if k > 0:
+            send(att.at[k], heads_y.at[own_seq], y_sent, y_sem, at(sources[k]))
+    heads_y[own_seq] = att[0]
+    if seqs > 1:
+        landed(heads_y.at[pl.ds(0, seqs - 1)], y_sem)
+    for d in range(1, tp_n):
+        to = lax.rem(tp + d, tp_n)
+        send(heads_y.at[:, to], heads_in.at[tp], x_sent, x_sem, {"tp": to})
+    heads_in[tp] = heads_y[:, tp]
+    landed(ow_all.at[pl.ds(0, tp_n - 1), 0], ow_sib)
+    landed(heads_in.at[pl.ds(0, tp_n - 1)], x_sem)
+
+    rows, width = res_ref.shape
+    each = rows // seqs
+    lhs = jnp.concatenate(
+        [heads_in[h].astype(jnp.float32).reshape(rows, LANES).astype(jnp.bfloat16) for h in range(tp_n)], axis=1
+    )
+    r_out = lax.broadcasted_iota(jnp.int32, (rows, rows), 0)
+    r_in = lax.broadcasted_iota(jnp.int32, (rows, rows), 1)
+    shuffle = (r_in == lax.rem(r_out, seqs) * each + r_out // seqs).astype(jnp.float32).astype(jnp.bfloat16)
+    lhs = jnp.dot(shuffle, lhs, preferred_element_type=jnp.float32).astype(jnp.bfloat16)
+    squares = 0.0
+    tile = 2 * LANES
+    for j in range(width // tile):
+        cols = slice(j * tile, (j + 1) * tile)
+        weight = ow_all[:, :, :, cols].reshape(lhs.shape[1], tile)
+        summed = res_ref[:, cols].astype(jnp.float32) + jnp.dot(lhs, weight, preferred_element_type=jnp.float32)
+        rounded = summed.astype(jnp.bfloat16)
+        stream_ref[:, cols] = rounded
+        wide = rounded.astype(jnp.float32)
+        squares = squares + jnp.sum(wide * wide, axis=1, keepdims=True)
+    scale = lax.rsqrt(squares / width + epsilon)
+    for j in range(width // tile):
+        cols = slice(j * tile, (j + 1) * tile)
+        normed_ref[:, cols] = (stream_ref[:, cols].astype(jnp.float32) * scale * gain_ref[:, cols]).astype(jnp.bfloat16)
+
+    landed(kv_all.at[pl.ds(0, 4 * side - 1)], kv_sent)
+    if seqs > 1:
+        landed(q_all.at[pl.ds(0, seqs - 1)], q_sent)
+        landed(att.at[pl.ds(0, side - 1)], y_sent)
+    if half_ring > 1:
+        landed(ow_all.at[pl.ds(0, 2 * (half_ring - 1)), 0], ow_sent)
+    landed(ow_all.at[0, 0], ow_half)
+    landed(ow_all.at[pl.ds(0, tp_n - 1), 0], ow_sib_sent)
+    landed(heads_in.at[pl.ds(0, tp_n - 1)], x_sent)
+
+
+def attention(sp_n, tp_n, queries, keyed, out_weight, residual, norm_gain):
+    seqs, positions, _ = queries.shape
+    rows, width = residual.shape
+    side = sp_n // 4
+    each = positions // tp_n
+    vmem = pl.BlockSpec(memory_space=pltpu.VMEM)
+    dma = pltpu.SemaphoreType.DMA
+    bf16, f32 = jnp.bfloat16, jnp.float32
+    return pl.pallas_call(
+        functools.partial(attention_kernel, sp_n, tp_n, seqs),
+        out_shape=[jax.ShapeDtypeStruct((rows, width), bf16)] * 2,
+        in_specs=[vmem] * 5,
+        out_specs=[vmem] * 2,
+        scratch_shapes=[
+            pltpu.VMEM((4 * side,) + keyed.shape[1:], bf16),
+            pltpu.VMEM((side,) + queries.shape[1:], bf16),
+            pltpu.VMEM((tp_n, 2, out_weight.shape[0] // 2, width), bf16),
+            pltpu.VMEM((side, tp_n, each, LANES), bf16),
+            pltpu.VMEM((seqs, tp_n, each, LANES), bf16),
+            pltpu.VMEM((tp_n, seqs, each, LANES), bf16),
+            pltpu.VMEM((side, positions, LANES), f32),
+            pltpu.VMEM((side, positions, LANES), f32),
+            pltpu.VMEM((side, positions, LANES), f32),
+            dma((side,)), dma((side,)), dma((2, side)), dma((side,)), dma((2, tp_n // 2)),
+            dma, dma, dma, dma, dma, dma, dma, dma, dma, dma,
+        ],
+        compiler_params=pltpu.CompilerParams(collective_id=2, has_side_effects=True),
+        name="attention",
+    )(queries, keyed, out_weight, residual, norm_gain)
+
+
+def prepared(query, latent, rope_key, latent_gain, key_up, value_up, own_positions):
+    seqs = query.shape[1]
+    half = query.shape[0] // 2
+    by_seq = query.transpose(1, 0, 2)
+    turned = rotate_by(by_seq[..., NOPE:].astype(jnp.float32), own_positions).astype(jnp.bfloat16)
+    queries = jnp.concatenate([by_seq[..., :NOPE], turned, turned], axis=-1)
+    rows = latent.transpose(1, 0, 2)
+    normed = rms_scale(rows.astype(jnp.float32), latent_gain).astype(jnp.bfloat16)
+    keys = jnp.dot(normed, key_up, preferred_element_type=jnp.float32).astype(jnp.bfloat16)
     values = jnp.dot(normed, value_up, preferred_element_type=jnp.float32).astype(jnp.bfloat16)
-    lead = latent_rows.shape[:2]
-    return (
-        keys_nope.reshape(lead + (key_up.shape[1] // NOPE, NOPE)),
-        values.reshape(lead + (value_up.shape[1] // VDIM, VDIM)),
-    )
-
-
-def absorb(carried, query_nope, query_rot, key_nope, value_rows, key_rot):
-    running, totals, accumulated = carried
-    scores = jnp.einsum("qshd,kshd->qshk", query_nope, key_nope, preferred_element_type=jnp.float32)
-    scores = scores + jnp.einsum(
-        "qshd,ksd->qshk", query_rot, key_rot, preferred_element_type=jnp.float32
-    )
-    scores = scores * QK ** (-0.5)
-    highest = jnp.maximum(running, jnp.max(scores, axis=-1))
-    weights = jnp.exp(scores - highest[..., None])
-    totals = jnp.sum(weights, axis=-1)
-    accumulated = jnp.einsum(
-        "qshk,kshd->qshd",
-        weights.astype(jnp.bfloat16),
-        value_rows,
-        preferred_element_type=jnp.float32,
-    )
-    return (highest, totals, accumulated)
+    key_rot = rotate_by(rope_key.transpose(1, 0, 2).astype(jnp.float32), own_positions).astype(jnp.bfloat16)
+    packed = jnp.concatenate([key_rot[:, :half], key_rot[:, half:]], axis=-1)
+    return queries, jnp.concatenate([keys, values, packed], axis=1)
 
 
 def moe_kernel(sp_n, tp_n, normed_ref, stream_ref, routes_ref, mix_ref, wg_hbm, wu_hbm, wd_hbm, out_ref,
@@ -266,36 +469,20 @@
     w_down,
 ):
     positions_here = query.shape[0]
-    heads_here = key_up.shape[1] // NOPE
     own_positions = lax.axis_index("sp") * positions_here + jnp.arange(
         positions_here, dtype=jnp.int32
     )
-    split_query = query.reshape(positions_here, SEQS, heads_here, QK)
-    query_nope = split_query[..., :NOPE]
-    query_rot = rotate(split_query[..., NOPE:].astype(jnp.float32), own_positions).astype(
-        jnp.bfloat16
-    )
-    key_rot = rotate(rope_key.astype(jnp.float32), own_positions).astype(jnp.bfloat16)
-    initial = (
-        jnp.full((positions_here, SEQS, heads_here), lowest, jnp.float32),
-        jnp.zeros((positions_here, SEQS, heads_here), jnp.float32),
-        jnp.zeros((positions_here, SEQS, heads_here, VDIM), jnp.float32),
-    )
-    own_keys, own_values = expand(latent, latent_gain, key_up, value_up)
-    pieces = side_by_side((own_keys, own_values, key_rot), "sp", 0, 2)
-    finished = absorb(initial, query_nope, query_rot, pieces[0], pieces[1], pieces[2])
-    attended = (finished[2] / finished[1][..., None]).astype(jnp.bfloat16)
-    attended = attended.reshape(positions_here, SEQS, heads_here * VDIM)
-    by_token = lax.all_to_all(attended, "tp", split_axis=0, concat_axis=2, tiled=True)
-    row_count = by_token.shape[0] * SEQS
-    mixed_heads = by_token.reshape(row_count, by_token.shape[2])
-    projected = jnp.dot(
-        mixed_heads,
-        lax.all_gather(out_weight, "tp", axis=0, tiled=True),
-        preferred_element_type=jnp.float32,
-    )
-    stream = (residual.reshape(row_count, D).astype(jnp.float32) + projected).astype(jnp.bfloat16)
-    normed = rms_scale(stream.astype(jnp.float32), norm_gain).astype(jnp.bfloat16)
+    row_count = residual.shape[0] * residual.shape[1]
+    queries, keyed = prepared(query, latent, rope_key, latent_gain, key_up, value_up, own_positions)
+    stream, normed = attention(
+        lax.axis_size("sp"),
+        lax.axis_size("tp"),
+        queries,
+        keyed,
+        out_weight,
+        residual.reshape(row_count, D),
+        norm_gain.reshape(1, D),
+    )
     mixing = jax.nn.softmax(pair_logits.reshape(row_count, TOPK), axis=-1) * group_prob.reshape(
         row_count, 1
     )

time: 275 us -> 187 us (0.68); the launches traced: 274 us -> 183 us
  waiting for transfers between devices: 120 us -> 0 us
  Pallas kernels: 107 us -> 172 us
  between operations: 13.7 us -> 0.17 us
  matrix products: 14.2 us -> 0.87 us
  starting transfers between devices: 6.49 us -> 0 us
  other arithmetic: 8.28 us -> 2.89 us
    all_gather x2 -> x0, waiting for transfers between devices: 108 us -> none  [the longest x1 80.4 us: side_by_side(): out = lax.all_gather(both, axis, axis=dim, tiled=True)]
    pallas_call x0 -> x1, Pallas kernels: none -> 72.2 us  [attention(): pl.pallas_call(functools.partial(attention_kernel, sp_n, tp_n, seqs), out...]
    dot_general x6 -> x2, matrix products: 14.2 us -> 0.87 us  [the longest x1 0.44 us: prepared(): jnp.dot(normed, value_up, preferred_element_type=jnp.float32)]
    all_to_all x1 -> x0, waiting for transfers between devices: 10.6 us -> none  [shards(): lax.all_to_all(attended, 'tp', split_axis=0, concat_axis=2, tiled=True)]
    pallas_call x1, Pallas kernels: 107 us -> 99.8 us  [routed_experts(): pl.pallas_call(functools.partial(moe_kernel, sp_n, tp_n), out_shape=jax.S...]
    all_to_all x1 -> x0, starting transfers between devices: 6.42 us -> none  [shards(): lax.all_to_all(attended, 'tp', split_axis=0, concat_axis=2, tiled=True)]
  transfers between devices with their start and end apart: 3 -> 0, of which waited for: 3 -> 0; matrix products, arithmetic and copies ran while one was open for 6% -> 0% of each run, Pallas kernels for 0% -> 0%
where the time goes in v2:
time: 187 us; the launch traced here: 183 us
  Pallas kernels  172 us (92%)
  local copies, waits for them, and re-layouts  7.45 us (4%)
  other arithmetic  2.89 us (2%)
    pallas_call x1, Pallas kernels, routed_experts(): pl.pallas_call(functools.partial(moe_kernel, sp_n, tp_n), out_shape=jax.S...  99.8 us
    pallas_call x1, Pallas kernels, attention(): pl.pallas_call(functools.partial(attention_kernel, sp_n, tp_n, seqs), out...  72.2 us

profile of v2, /device:TPU:513, one launch (start us, length us, event | category | flops | bytes accessed | tf_op | source)
XLA Modules:
  0.0 183.4 jit_solution(4270127644119216383)
XLA Ops:
  0.0 1.1 copy.55
  1.1 1.0 copy.43
  2.2 0.4 multiply_cosine_fusion
  2.7 0.4 subtract_convert_fusion
  3.0 1.1 concatenate.16.q_ref
  4.2 0.1 fusion.15
  4.3 0.3 fusion
  4.6 0.4 convolution_convert_fusion
  5.1 0.0 copy-done.6
  5.1 0.4 convolution_convert_fusion.1
  5.5 0.9 fusion.12.kv_ref
  6.4 0.9 reshape.103.res_ref
  7.3 72.2 %attention.1 = (bf16[96,2048]{1,0:T(8,128)(2,1)}, bf16[96,2048]{1,0:T(8,128)(2,1)}) custom-call(bf16[4,192,256]{2,1,0:T(8,128)(2,1)} %concatenate.16.q_ref, bf16[4,480,128]{2,1,0:T(8,128)(2,1)} %fusion.12.kv_ref, bf16[128,2048]{1,0:T(8,128)(2,1)} %ow_ref.1, bf16[96,2048]{1,0:T(8,128)(2,1)} %reshape.103.res_ref, f32[1,2048]{1,0:T(1,128)} %bitcast.35), custom_call_target="tpu_custom_call" | custom-call | tf_op jit(solution)/shard_map/attention/pallas_call | solution.py:258
  79.5 0.7 copy.44
  80.2 0.1 copy.45
  80.4 0.1 copy.46
  80.4 0.1 sub.23
  80.6 0.1 copy.49
  80.6 0.1 mul.130
  80.8 0.1 copy.48
  80.9 0.1 div.23
  81.0 0.7 divide_multiply_fusion.mix_ref
  81.7 99.8 %routed_experts.1 = bf16[96,2048]{1,0:T(8,128)(2,1)} custom-call(bf16[96,2048]{1,0:T(8,128)(2,1)} %get-tuple-element.7.normed_ref, bf16[96,2048]{1,0:T(8,128)(2,1)} %get-tuple-element.8.stream_ref, s32[96,2]{1,0:T(8,128)} %bitcast.33, f32[96,2]{1,0:T(8,128)} %divide_multiply_fusion.mix_ref, bf16[2048,768]{1,0:T(8,128)(2,1)} %bitcast.28, ...), custom_call_target="tpu_custom_call" | custom-call | tf_op jit(solution)/shard_map/routed_experts/pallas_call | solution.py:435
  181.5 1.9 %reshape.107 = bf16[24,4,2048]{2,1,0:T(4,128)(2,1)} reshape(bf16[96,2048]{1,0:T(8,128)(2,1)} %routed_experts.1) | data formatting | bytes 786432 | tf_op jit(solution)/shard_map/reshape | solution.py:500
  (22 shorter events, 0.2 us)
Async XLA Ops:
  0.0 4.6 %copy-start = (bf16[512,128]{1,0:T(8,128)(2,1)S(1)}, bf16[512,128]{1,0:T(8,128)(2,1)}, u32[]{:S(2)}) copy-start(bf16[512,128]{1,0:T(8,128)(2,1)} %param.21) | copy-start | bytes 393220
  3.0 1.3 copy-start.1
  3.0 1.6 copy-start.7
  4.2 0.9 copy-start.6
  5.1 1.4 copy-start.2
  6.4 73.1 %copy-start.4 = (s32[24,4,2]{0,2,1:T(2,128)S(1)}, s32[24,4,2]{0,2,1:T(2,128)}, u32[]{:S(2)}) copy-start(s32[24,4,2]{0,2,1:T(2,128)} %param.26) | copy-start | bytes 2308
  6.4 73.8 %copy-start.3 = (f32[24,4,2]{0,2,1:T(2,128)S(1)}, f32[24,4,2]{0,2,1:T(2,128)}, u32[]{:S(2)}) copy-start(f32[24,4,2]{0,2,1:T(2,128)} %param.25) | copy-start | bytes 2308
  6.4 74.1 %copy-start.5 = (f32[24,4]{0,1:T(4,128)S(1)}, f32[24,4]{0,1:T(4,128)}, u32[]{:S(2)}) copy-start(f32[24,4]{0,1:T(4,128)} %param.24) | copy-start | bytes 1156

commit v3 on v2

--- a/solution.py
+++ b/solution.py
@@ -294,29 +294,133 @@
 
 
 def moe_kernel(sp_n, tp_n, normed_ref, stream_ref, routes_ref, mix_ref, wg_hbm, wu_hbm, wd_hbm, out_ref,
-               wg, wu, wd, stage, outgoing, arrived, leaving, returned, rows_in, w_sems, send_sem, recv_sem, back_send, back_recv):
+               wg, wu, wd, stage, rows_in, w_sems, *scratch):
+    chips = sp_n // 2
     peers = sp_n * tp_n
+    plane = chips * tp_n
     rows, width = normed_ref.shape
     chunks = width // LANES
+    span = CAP * chunks
     sp, tp = lax.axis_index("sp"), lax.axis_index("tp")
-    me = sp * tp_n + tp
+    chip, core = sp // 2, lax.rem(sp, 2)
     barrier = pltpu.get_barrier_semaphore()
-
-    def peer(i):
-        other = lax.rem(me + i, peers)
-        return other, {"sp": other // tp_n, "tp": lax.rem(other, tp_n)}
-
-    def greet(i, _):
-        pl.semaphore_signal(barrier, inc=1, device_id=peer(i)[1], device_id_type=MESH)
-        return 0
-
-    lax.fori_loop(1, peers, greet, 0)
+    sibling = {"sp": 2 * chip + 1 - core}
+
+    def across(d):
+        to = lax.rem(tp + d, tp_n)
+        return to, {"tp": to}
+
+    def along(d):
+        to = lax.rem(chip + d, chips)
+        return to, {"sp": 2 * to + core}
+
+    ring = []
+    for d in range(1, max(chips, tp_n) // 2 + 1):
+        for step in (d, -d):
+            if d < tp_n and (step > 0 or 2 * d != tp_n) and d <= tp_n // 2:
+                ring.append((across, step % tp_n))
+            if d < chips and (step > 0 or 2 * d != chips) and d <= chips // 2:
+                ring.append((along, step % chips))
+    for where in [sibling] + [way(d)[1] for way, d in ring]:
+        pl.semaphore_signal(barrier, inc=1, device_id=where, device_id_type=MESH)
     loads = [
         pltpu.make_async_copy(src, dst, w_sems.at[k])
         for k, (src, dst) in enumerate(((wg_hbm, wg), (wu_hbm, wu), (wd_hbm, wd)))
     ]
     for load in loads:
         load.start()
+
+    def send(src, dst, sent, got, where):
+        pltpu.make_async_remote_copy(
+            src_ref=src, dst_ref=dst, send_sem=sent, recv_sem=got, device_id=where, device_id_type=MESH
+        ).start()
+
+    def landed(buffer, sem):
+        pltpu.make_async_copy(buffer, buffer, sem).wait()
+
+    def exchange(buffers):
+        held, given, by_tp, by_sp, from_even, from_odd, sems = buffers
+
+        def even_first():
+            for way, d in ring:
+                if way is across:
+                    to, where = across(d)
+                    send(held.at[0, pl.ds(to * chips, chips)], by_tp.at[tp], sems.at[0], sems.at[1], where)
+
+        def odd_first():
+            for way, d in ring:
+                if way is along:
+                    to, where = along(d)
+                    send(held.at[1, pl.ds(to * tp_n, tp_n)], by_sp.at[chip], sems.at[2], sems.at[3], where)
+
+        send(given, held.at[core], sems.at[8], sems.at[9], sibling)
+        pl.when(core == 0)(even_first)
+        pl.when(core == 1)(odd_first)
+        landed(given, sems.at[9])
+        pl.when(core == 1)(even_first)
+        pl.when(core == 0)(odd_first)
+        by_tp[tp] = held[0, pl.ds(tp * chips, chips)]
+        by_sp[chip] = held[1, pl.ds(chip * tp_n, tp_n)]
+        landed(by_tp.at[pl.ds(0, tp_n - 1)], sems.at[1])
+        for way, d in ring:
+            if way is along:
+                to, where = along(d)
+                send(by_tp.at[:, to], from_even.at[chip], sems.at[4], sems.at[5], where)
+        landed(by_sp.at[pl.ds(0, chips - 1)], sems.at[3])
+        for way, d in ring:
+            if way is across:
+                to, where = across(d)
+                send(by_sp.at[:, to], from_odd.at[tp], sems.at[6], sems.at[7], where)
+        from_even[chip] = by_tp[:, chip]
+        from_odd[tp] = by_sp[:, tp]
+        landed(from_even.at[pl.ds(0, chips - 1)], sems.at[5])
+        landed(from_odd.at[pl.ds(0, tp_n - 1)], sems.at[7])
+
+    def sent(buffers):
+        held, given, by_tp, by_sp, from_even, from_odd, sems = buffers
+        landed(given, sems.at[8])
+        landed(by_tp.at[pl.ds(0, tp_n - 1)], sems.at[0])
+        landed(by_sp.at[pl.ds(0, chips - 1)], sems.at[2])
+        landed(from_even.at[pl.ds(0, chips - 1)], sems.at[4])
+        landed(from_odd.at[pl.ds(0, tp_n - 1)], sems.at[6])
+
+    step = min(8, plane)
+
+    def pack(buffers, place):
+        held, given = buffers[:2]
+
+        def block(i, to_core):
+            c = lax.rem(i, chips) * (1 - core) + i // tp_n * core
+            x = i // chips * (1 - core) + lax.rem(i, tp_n) * core
+            return stage[pl.ds(pl.multiple_of(place(c, to_core, x) * span, span), span), :].astype(jnp.bfloat16)
+
+        def body(n, _):
+            for j in range(step):
+                i = n * step + j
+                held[core, i] = block(i, core)
+                given[i] = block(i, 1 - core)
+            return 0
+
+        lax.fori_loop(0, plane // step, body, 0)
+
+    def unpack(buffers, place):
+        from_even, from_odd = buffers[4:6]
+
+        def put(where, block):
+            stage[pl.ds(pl.multiple_of(where * span, span), span), :] = block.astype(jnp.float32)
+
+        def body(n, _):
+            for j in range(step):
+                i = n * step + j
+                c, x = i // tp_n, lax.rem(i, tp_n)
+                put(place(c, 0, x), from_even[c, x])
+                put(place(c, 1, x), from_odd[x, c])
+            return 0
+
+        lax.fori_loop(0, plane // step, body, 0)
+
+    def device(c, core_id, x):
+        return (2 * c + core_id) * tp_n + x
 
     experts = lax.broadcasted_iota(jnp.int32, (rows, peers), 1)
     picks = [(routes_ref[:, k : k + 1] == experts).astype(jnp.float32) for k in range(TOPK)]
@@ -339,52 +443,17 @@
         )
         for c in range(CAP):
             for h in range(2):
-                stage[pl.ds(c * chunks + 2 * j + h, peers, stride=CAP * chunks), :] = part[
+                stage[pl.ds(c * chunks + 2 * j + h, peers, stride=span), :] = part[
                     c * peers : (c + 1) * peers, h * LANES : (h + 1) * LANES
                 ]
-    step = min(8, peers)
-    span = CAP * chunks
-
-    def pack(dst):
-        def body(i, _):
-            rows_at = pl.ds(pl.multiple_of(i * step * span, step * span), step * span)
-            dst[pl.ds(i * step, step)] = stage[rows_at, :].astype(jnp.bfloat16).reshape(step, span, LANES)
-            return 0
-
-        lax.fori_loop(0, peers // step, body, 0)
-
-    def unpack(src):
-        def body(i, _):
-            rows_at = pl.ds(pl.multiple_of(i * step * span, step * span), step * span)
-            stage[rows_at, :] = src[pl.ds(i * step, step)].astype(jnp.float32).reshape(step * span, LANES)
-            return 0
-
-        lax.fori_loop(0, peers // step, body, 0)
-
-    def exchange(src, dst, sent, got):
-        def body(i, _):
-            other, where = peer(i)
-            pltpu.make_async_remote_copy(
-                src_ref=src.at[other], dst_ref=dst.at[me], send_sem=sent, recv_sem=got, device_id=where,
-                device_id_type=MESH,
-            ).start()
-            return 0
-
-        lax.fori_loop(1, peers, body, 0)
-        dst[me] = src[me]
-
-    def settle(buffer, sem):
-        many = buffer.at[pl.ds(0, peers - 1)]
-        pltpu.make_async_copy(many, many, sem).wait()
-
-    pack(outgoing)
-    pl.semaphore_wait(barrier, peers - 1)
-    exchange(outgoing, arrived, send_sem, recv_sem)
+    there, back = scratch[:7], scratch[7:]
+    pack(there, device)
+    pl.semaphore_wait(barrier, len(ring) + 1)
+    exchange(there)
     for load in loads:
         load.wait()
-    settle(arrived, recv_sem)
-
-    unpack(arrived)
+
+    unpack(there, device)
     total = peers * CAP
     for l in range(chunks):
         rows_in[:, l * LANES : (l + 1) * LANES] = stage[pl.ds(l, total, stride=chunks), :].astype(jnp.bfloat16)
@@ -400,12 +469,10 @@
         part = jnp.dot(hidden, wd[:, 2 * j * LANES : (2 * j + 2) * LANES], preferred_element_type=jnp.float32)
         for h in range(2):
             stage[pl.ds(2 * j + h, total, stride=chunks), :] = part[:, h * LANES : (h + 1) * LANES]
-    pack(leaving)
-    exchange(leaving, returned, back_send, back_recv)
-    settle(outgoing, send_sem)
-    settle(returned, back_recv)
-
-    unpack(returned)
+    pack(back, device)
+    exchange(back)
+
+    unpack(back, device)
     for j in range(chunks // 2):
         block = jnp.concatenate(
             [
@@ -421,17 +488,26 @@
             :, 1:2
         ] * jnp.dot(chosen[1], block, preferred_element_type=jnp.float32)
         out_ref[:, cols] = (stream_ref[:, cols].astype(jnp.float32) + added).astype(jnp.bfloat16)
-    settle(leaving, back_send)
+    sent(there)
+    sent(back)
 
 
 def routed_experts(sp_n, tp_n, normed, stream, routes, mixing, w_gate, w_up, w_down):
     rows, width = normed.shape
     peers = sp_n * tp_n
+    chips = sp_n // 2
     span = CAP * width // LANES
     vmem = pl.BlockSpec(memory_space=pltpu.VMEM)
     hbm = pl.BlockSpec(memory_space=pl.ANY)
-    blocks = pltpu.VMEM((peers, span, LANES), jnp.bfloat16)
     dma = pltpu.SemaphoreType.DMA
+
+    def blocks(*lead):
+        return pltpu.VMEM((*lead, span, LANES), jnp.bfloat16)
+
+    buffers = [
+        blocks(2, chips * tp_n), blocks(chips * tp_n), blocks(tp_n, chips), blocks(chips, tp_n), blocks(chips, tp_n),
+        blocks(tp_n, chips), dma((10,)),
+    ]
     return pl.pallas_call(
         functools.partial(moe_kernel, sp_n, tp_n),
         out_shape=jax.ShapeDtypeStruct((rows, width), jnp.bfloat16),
@@ -442,9 +518,10 @@
             pltpu.VMEM(w_up.shape, jnp.bfloat16),
             pltpu.VMEM(w_down.shape, jnp.bfloat16),
             pltpu.VMEM((peers * span, LANES), jnp.float32),
-            blocks, blocks, blocks, blocks,
             pltpu.VMEM((peers * CAP, width), jnp.bfloat16),
-            dma((3,)), dma, dma, dma, dma,
+            dma((3,)),
+            *buffers,
+            *buffers,
         ],
         compiler_params=pltpu.CompilerParams(collective_id=1, has_side_effects=True),
         name="routed_experts",

time: 187 us -> 158 us (0.84); the launches traced: 183 us -> 157 us
  Pallas kernels: 172 us -> 146 us
    pallas_call x1, Pallas kernels: 99.8 us -> 73.6 us  [routed_experts(): pl.pallas_call(functools.partial(moe_kernel, sp_n, tp_n), out_shape=jax.S...]
where the time goes in v3:
time: 158 us; the launch traced here: 157 us
  Pallas kernels  146 us (92%)
  local copies, waits for them, and re-layouts  7.45 us (5%)
  other arithmetic  2.89 us (2%)
    pallas_call x1, Pallas kernels, routed_experts(): pl.pallas_call(functools.partial(moe_kernel, sp_n, tp_n), out_shape=jax.S...  73.6 us
    pallas_call x1, Pallas kernels, attention(): pl.pallas_call(functools.partial(attention_kernel, sp_n, tp_n, seqs), out...  72.2 us

profile of v3, /device:TPU:513, one launch (start us, length us, event | category | flops | bytes accessed | tf_op | source)
XLA Modules:
  0.0 157.2 jit_solution(6914356666892549588)
XLA Ops:
  0.0 1.1 copy.55
  1.1 1.0 copy.43
  2.2 0.4 multiply_cosine_fusion
  2.7 0.4 subtract_convert_fusion
  3.0 1.1 concatenate.16.q_ref
  4.2 0.1 fusion.15
  4.3 0.3 fusion
  4.6 0.4 convolution_convert_fusion
  5.1 0.0 copy-done.6
  5.1 0.4 convolution_convert_fusion.1
  5.5 0.9 fusion.12.kv_ref
  6.4 0.9 reshape.103.res_ref
  7.3 72.2 %attention.1 = (bf16[96,2048]{1,0:T(8,128)(2,1)}, bf16[96,2048]{1,0:T(8,128)(2,1)}) custom-call(bf16[4,192,256]{2,1,0:T(8,128)(2,1)} %concatenate.16.q_ref, bf16[4,480,128]{2,1,0:T(8,128)(2,1)} %fusion.12.kv_ref, bf16[128,2048]{1,0:T(8,128)(2,1)} %ow_ref.1, bf16[96,2048]{1,0:T(8,128)(2,1)} %reshape.103.res_ref, f32[1,2048]{1,0:T(1,128)} %bitcast.35), custom_call_target="tpu_custom_call" | custom-call | tf_op jit(solution)/shard_map/attention/pallas_call | solution.py:258
  79.5 0.7 copy.44
  80.2 0.1 copy.45
  80.4 0.1 copy.46
  80.4 0.1 sub.23
  80.6 0.1 copy.49
  80.6 0.1 mul.130
  80.8 0.1 copy.48
  80.9 0.1 div.23
  81.0 0.7 divide_multiply_fusion.mix_ref
  81.7 73.6 %routed_experts.1 = bf16[96,2048]{1,0:T(8,128)(2,1)} custom-call(bf16[96,2048]{1,0:T(8,128)(2,1)} %get-tuple-element.7.normed_ref, bf16[96,2048]{1,0:T(8,128)(2,1)} %get-tuple-element.8.stream_ref, s32[96,2]{1,0:T(8,128)} %bitcast.33, f32[96,2]{1,0:T(8,128)} %divide_multiply_fusion.mix_ref, bf16[2048,768]{1,0:T(8,128)(2,1)} %bitcast.28, ...), custom_call_target="tpu_custom_call" | custom-call | tf_op jit(solution)/shard_map/routed_experts/pallas_call | solution.py:511
  155.3 1.9 %reshape.107 = bf16[24,4,2048]{2,1,0:T(4,128)(2,1)} reshape(bf16[96,2048]{1,0:T(8,128)(2,1)} %routed_experts.1) | data formatting | bytes 786432 | tf_op jit(solution)/shard_map/reshape | solution.py:577
  (22 shorter events, 0.2 us)
Async XLA Ops:
  0.0 4.6 %copy-start = (bf16[512,128]{1,0:T(8,128)(2,1)S(1)}, bf16[512,128]{1,0:T(8,128)(2,1)}, u32[]{:S(2)}) copy-start(bf16[512,128]{1,0:T(8,128)(2,1)} %param.21) | copy-start | bytes 393220
  3.0 1.3 copy-start.1
  3.0 1.6 %copy-start.7 = (f32[512]{0:T(512)S(1)}, f32[512]{0:T(512)}, u32[]{:S(2)}) copy-start(f32[512]{0:T(512)} %param.19) | copy-start | bytes 6148
  4.2 0.9 copy-start.6
  5.1 1.4 copy-start.2
  6.4 73.1 %copy-start.4 = (s32[24,4,2]{0,2,1:T(2,128)S(1)}, s32[24,4,2]{0,2,1:T(2,128)}, u32[]{:S(2)}) copy-start(s32[24,4,2]{0,2,1:T(2,128)} %param.26) | copy-start | bytes 2308
  6.4 73.8 %copy-start.3 = (f32[24,4,2]{0,2,1:T(2,128)S(1)}, f32[24,4,2]{0,2,1:T(2,128)}, u32[]{:S(2)}) copy-start(f32[24,4,2]{0,2,1:T(2,128)} %param.25) | copy-start | bytes 2308
  6.4 74.1 %copy-start.5 = (f32[24,4]{0,1:T(4,128)S(1)}, f32[24,4]{0,1:T(4,128)}, u32[]{:S(2)}) copy-start(f32[24,4]{0,1:T(4,128)} %param.24) | copy-start | bytes 1156

commit v4 on v3

--- a/solution.py
+++ b/solution.py
@@ -13,6 +13,7 @@
 QK = 192
 TOPK = 2
 CAP = 2
+PARTS = 2
 LANES = 128
 MESH = pl.DeviceIdType.MESH
 
@@ -55,8 +56,8 @@
     sp, tp = lax.axis_index("sp"), lax.axis_index("tp")
     chip, core = sp // 2, lax.rem(sp, 2)
     own_seq, own_g = chip // 2, lax.rem(chip, 2)
-    positions = q_ref.shape[1]
-    half = positions // 2
+    half = q_ref.shape[1] // 3
+    positions = 2 * half
     part = ow_ref.shape[0] // 2
 
     def at(chip_id, core_id=None):
@@ -95,7 +96,6 @@
     own_slot = slot(core, own_g, 0)
     for seq, g, home, k in homes:
         send(kv_ref.at[seq], kv_all.at[slot(core, g, k)], kv_sent, kv_sem.at[k], at(home))
-        send(q_ref.at[seq], q_all.at[k], q_sent, q_sem.at[k], at(home))
 
     def ow_stage(r):
         for way, to in ((0, right), (1, left)):
@@ -125,31 +125,35 @@
         send(src, place, kv_sent, kv_fwd.at[k], at(beside))
         send(src, place, kv_sent, kv_sib.at[own_g, k], at(chip, 1 - core))
 
+    pass_on(0, kv_ref.at[own_seq])
     ow_stage(1)
-    pass_on(0, kv_ref.at[own_seq])
+    for seq, g, home, k in homes:
+        send(q_ref.at[seq], q_all.at[k], q_sent, q_sem.at[k], at(home))
     kv_all[own_slot] = kv_ref[own_seq]
     q_all[0] = q_ref[own_seq]
     ow_all[tp] = ow_ref[...].reshape(ow_all.shape[1:])
 
-    lane = lax.broadcasted_iota(jnp.int32, (positions, 2 * LANES), 1)
-    low = lane < LANES + LANES // 2
-    high = (lane < LANES) | (lane >= LANES + LANES // 2)
+    low = lax.broadcasted_iota(jnp.int32, (half, LANES), 1) < LANES // 2
     factor = QK ** (-0.5) * math.log2(math.e)
 
     def attend(base, k, first, last):
         def rows(start):
             return kv_all[pl.ds(base, side), start : start + half, :].reshape(side * half, LANES)
 
-        q = q_all[k]
+        plain = q_all[k, :positions]
+        first_rot = q_all[k, positions:].astype(jnp.float32)
+        second_rot = pltpu.roll(first_rot, LANES // 2, 1)
+        halves = [
+            jnp.concatenate([jnp.where(low, first_rot, 0.0), jnp.where(low, second_rot, 0.0)], axis=0),
+            jnp.concatenate([jnp.where(low, 0.0, second_rot), jnp.where(low, 0.0, first_rot)], axis=0),
+        ]
         turned = rows(4 * half)
         scores = []
-        for n, mask in ((0, low), (1, high)):
+        for n in range(2):
             keys = jnp.concatenate([rows(n * half), turned], axis=1)
+            q = jnp.concatenate([plain, halves[n].astype(jnp.bfloat16)], axis=1)
             scores.append(
-                lax.dot_general(
-                    jnp.where(mask, q, jnp.zeros_like(q)), keys, (((1,), (1,)), ((), ())),
-                    preferred_element_type=jnp.float32,
-                )
+                lax.dot_general(q, keys, (((1,), (1,)), ((), ())), preferred_element_type=jnp.float32)
             )
         top = jnp.maximum(jnp.max(scores[0], axis=1, keepdims=True), jnp.max(scores[1], axis=1, keepdims=True))
         if not first:
@@ -178,37 +182,51 @@
 
         lax.fori_loop(0, side, body, 0)
 
+    def direct_arrived(k):
+        place = kv_all.at[slot(core, own_g, k)]
+        landed(place, kv_sem.at[k])
+        pass_on(k, place)
+
+    def forward_arrived(k):
+        place = kv_all.at[slot(core, 1 - own_g, k)]
+        landed(place, kv_fwd.at[k])
+        send(place, place, kv_sent, kv_sib.at[1 - own_g, k], at(chip, 1 - core))
+
+    forward_arrived(0)
     for k in range(1, side):
-        landed(kv_all.at[slot(core, own_g, k)], kv_sem.at[k])
-        pass_on(k, kv_all.at[slot(core, own_g, k)])
-        if k < half_ring:
-            ow_arrived(k)
+        direct_arrived(k)
+        if k == 1:
+            ow_arrived(1)
+        forward_arrived(k)
+    for r in range(2, min(3, half_ring + 1)):
+        ow_arrived(r)
     for k in range(1, side):
         landed(q_all.at[k], q_sem.at[k])
     attend_all(slot(core, own_g, 0), True)
     for k in range(side):
         landed(kv_all.at[slot(1 - core, own_g, k)], kv_sib.at[own_g, k])
     attend_all(slot(1 - core, own_g, 0), False)
-    for k in range(side):
-        place = kv_all.at[slot(core, 1 - own_g, k)]
-        landed(place, kv_fwd.at[k])
-        send(place, place, kv_sent, kv_sib.at[1 - own_g, k], at(chip, 1 - core))
-    for r in range(min(side, half_ring), half_ring + 1):
+    for r in range(3, half_ring):
         ow_arrived(r)
     attend_all(slot(core, 1 - own_g, 0), False)
     for k in range(side):
         landed(kv_all.at[slot(1 - core, 1 - own_g, k)], kv_sib.at[1 - own_g, k])
-    for k in list(range(1, side)) + [0]:
+    for k in reversed(range(side)):
         attend(slot(1 - core, 1 - own_g, 0), k, False, True)
         if k > 0:
-            send(att.at[k], heads_y.at[own_seq], y_sent, y_sem, at(sources[k]))
-    heads_y[own_seq] = att[0]
-    if seqs > 1:
-        landed(heads_y.at[pl.ds(0, seqs - 1)], y_sem)
-    for d in range(1, tp_n):
-        to = lax.rem(tp + d, tp_n)
-        send(heads_y.at[:, to], heads_in.at[tp], x_sent, x_sem, {"tp": to})
-    heads_in[tp] = heads_y[:, tp]
+            send(att.at[k], heads_y.at[own_seq], y_sent, y_sem.at[own_seq], at(sources[k]))
+    for e in range(seqs):
+        seq, block = own_seq, att.at[0]
+        if e > 0:
+            seq = homes[e - 1][0]
+            block = heads_y.at[seq]
+            landed(block, y_sem.at[seq])
+        for d in range(1, tp_n):
+            to = lax.rem(tp + d, tp_n)
+            send(block.at[to], heads_in.at[tp, seq], x_sent, x_sem, {"tp": to})
+        heads_in[tp, seq] = block[tp]
+    if half_ring > 2:
+        ow_arrived(half_ring)
     landed(ow_all.at[pl.ds(0, tp_n - 1), 0], ow_sib)
     landed(heads_in.at[pl.ds(0, tp_n - 1)], x_sem)
 
@@ -248,7 +266,7 @@
 
 
 def attention(sp_n, tp_n, queries, keyed, out_weight, residual, norm_gain):
-    seqs, positions, _ = queries.shape
+    seqs, positions = queries.shape[0], queries.shape[1] // 3 * 2
     rows, width = residual.shape
     side = sp_n // 4
     each = positions // tp_n
@@ -271,7 +289,7 @@
             pltpu.VMEM((side, positions, LANES), f32),
             pltpu.VMEM((side, positions, LANES), f32),
             dma((side,)), dma((side,)), dma((2, side)), dma((side,)), dma((2, tp_n // 2)),
-            dma, dma, dma, dma, dma, dma, dma, dma, dma, dma,
+            dma, dma((seqs,)), dma, dma, dma, dma, dma, dma, dma, dma,
         ],
         compiler_params=pltpu.CompilerParams(collective_id=2, has_side_effects=True),
         name="attention",
@@ -283,7 +301,8 @@
     half = query.shape[0] // 2
     by_seq = query.transpose(1, 0, 2)
     turned = rotate_by(by_seq[..., NOPE:].astype(jnp.float32), own_positions).astype(jnp.bfloat16)
-    queries = jnp.concatenate([by_seq[..., :NOPE], turned, turned], axis=-1)
+    turned = jnp.concatenate([turned[:, :half], turned[:, half:]], axis=-1)
+    queries = jnp.concatenate([by_seq[..., :NOPE], turned], axis=1)
     rows = latent.transpose(1, 0, 2)
     normed = rms_scale(rows.astype(jnp.float32), latent_gain).astype(jnp.bfloat16)
     keys = jnp.dot(normed, key_up, preferred_element_type=jnp.float32).astype(jnp.bfloat16)
@@ -293,7 +312,7 @@
     return queries, jnp.concatenate([keys, values, packed], axis=1)
 
 
-def moe_kernel(sp_n, tp_n, normed_ref, stream_ref, routes_ref, mix_ref, wg_hbm, wu_hbm, wd_hbm, out_ref,
+def moe_kernel(sp_n, tp_n, normed_ref, stream_ref, small_ref, wg_hbm, wu_hbm, wd_hbm, out_ref,
                wg, wu, wd, stage, rows_in, w_sems, *scratch):
     chips = sp_n // 2
     peers = sp_n * tp_n
@@ -315,7 +334,7 @@
         return to, {"sp": 2 * to + core}
 
     ring = []
-    for d in range(1, max(chips, tp_n) // 2 + 1):
+    for d in reversed(range(1, max(chips, tp_n) // 2 + 1)):
         for step in (d, -d):
             if d < tp_n and (step > 0 or 2 * d != tp_n) and d <= tp_n // 2:
                 ring.append((across, step % tp_n))
@@ -338,51 +357,64 @@
     def landed(buffer, sem):
         pltpu.make_async_copy(buffer, buffer, sem).wait()
 
+    piece = span // PARTS
+
     def exchange(buffers):
-        held, given, by_tp, by_sp, from_even, from_odd, sems = buffers
+        held, given, by_tp, by_sp, from_even, from_odd, sems, swap = buffers
+
+        def part(p):
+            return pl.ds(p * piece, piece)
 
         def even_first():
-            for way, d in ring:
-                if way is across:
-                    to, where = across(d)
-                    send(held.at[0, pl.ds(to * chips, chips)], by_tp.at[tp], sems.at[0], sems.at[1], where)
+            for p in range(PARTS):
+                for way, d in ring:
+                    if way is across:
+                        to, where = across(d)
+                        src = held.at[0, pl.ds(to * chips, chips), part(p)]
+                        send(src, by_tp.at[tp, :, part(p)], sems.at[p, 0], sems.at[p, 1], where)
 
         def odd_first():
-            for way, d in ring:
-                if way is along:
-                    to, where = along(d)
-                    send(held.at[1, pl.ds(to * tp_n, tp_n)], by_sp.at[chip], sems.at[2], sems.at[3], where)
-
-        send(given, held.at[core], sems.at[8], sems.at[9], sibling)
+            for p in range(PARTS):
+                for way, d in ring:
+                    if way is along:
+                        to, where = along(d)
+                        src = held.at[1, pl.ds(to * tp_n, tp_n), part(p)]
+                        send(src, by_sp.at[chip, :, part(p)], sems.at[p, 2], sems.at[p, 3], where)
+
+        send(given, held.at[core], swap.at[0], swap.at[1], sibling)
         pl.when(core == 0)(even_first)
         pl.when(core == 1)(odd_first)
-        landed(given, sems.at[9])
+        landed(given, swap.at[1])
         pl.when(core == 1)(even_first)
         pl.when(core == 0)(odd_first)
         by_tp[tp] = held[0, pl.ds(tp * chips, chips)]
         by_sp[chip] = held[1, pl.ds(chip * tp_n, tp_n)]
-        landed(by_tp.at[pl.ds(0, tp_n - 1)], sems.at[1])
-        for way, d in ring:
-            if way is along:
-                to, where = along(d)
-                send(by_tp.at[:, to], from_even.at[chip], sems.at[4], sems.at[5], where)
-        landed(by_sp.at[pl.ds(0, chips - 1)], sems.at[3])
-        for way, d in ring:
-            if way is across:
-                to, where = across(d)
-                send(by_sp.at[:, to], from_odd.at[tp], sems.at[6], sems.at[7], where)
+        for p in range(PARTS):
+            landed(by_tp.at[pl.ds(0, tp_n - 1), :, part(p)], sems.at[p, 1])
+            for way, d in ring:
+                if way is along:
+                    to, where = along(d)
+                    send(by_tp.at[:, to, part(p)], from_even.at[chip, :, part(p)], sems.at[p, 4], sems.at[p, 5], where)
+            landed(by_sp.at[pl.ds(0, chips - 1), :, part(p)], sems.at[p, 3])
+            for way, d in ring:
+                if way is across:
+                    to, where = across(d)
+                    send(by_sp.at[:, to, part(p)], from_odd.at[tp, :, part(p)], sems.at[p, 6], sems.at[p, 7], where)
         from_even[chip] = by_tp[:, chip]
         from_odd[tp] = by_sp[:, tp]
-        landed(from_even.at[pl.ds(0, chips - 1)], sems.at[5])
-        landed(from_odd.at[pl.ds(0, tp_n - 1)], sems.at[7])
+        for p in range(PARTS):
+            landed(from_even.at[pl.ds(0, chips - 1), :, part(p)], sems.at[p, 5])
+            landed(from_odd.at[pl.ds(0, tp_n - 1), :, part(p)], sems.at[p, 7])
 
     def sent(buffers):
-        held, given, by_tp, by_sp, from_even, from_odd, sems = buffers
-        landed(given, sems.at[8])
-        landed(by_tp.at[pl.ds(0, tp_n - 1)], sems.at[0])
-        landed(by_sp.at[pl.ds(0, chips - 1)], sems.at[2])
-        landed(from_even.at[pl.ds(0, chips - 1)], sems.at[4])
-        landed(from_odd.at[pl.ds(0, tp_n - 1)], sems.at[6])
+        held, given, by_tp, by_sp, from_even, from_odd, sems, swap = buffers
+        landed(given, swap.at[0])
+        for p in range(PARTS):
+            part = pl.ds(p * piece, piece)
+            landed(by_tp.at[pl.ds(0, tp_n - 1), :, part], sems.at[p, 0])
+            landed(by_sp.at[pl.ds(0, chips - 1), :, part], sems.at[p, 2])
+            landed(from_even.at[pl.ds(0, chips - 1), :, part], sems.at[p, 4])
+            landed(from_odd.at[pl.ds(0, tp_n - 1), :, part], sems.at[p, 6])
 
     step = min(8, plane)
 
@@ -422,8 +454,14 @@
     def device(c, core_id, x):
         return (2 * c + core_id) * tp_n + x
 
-    experts = lax.broadcasted_iota(jnp.int32, (rows, peers), 1)
-    picks = [(routes_ref[:, k : k + 1] == experts).astype(jnp.float32) for k in range(TOPK)]
+    experts = lax.broadcasted_iota(jnp.int32, (rows, peers), 1).astype(jnp.float32)
+    small = small_ref[...]
+    picks = [(small[:, k : k + 1] == experts).astype(jnp.float32) for k in range(TOPK)]
+    logits = [small[:, TOPK + k : TOPK + k + 1] for k in range(TOPK)]
+    top = jnp.maximum(logits[0], logits[1])
+    raised = [jnp.exp(v - top) for v in logits]
+    shared = small[:, 2 * TOPK : 2 * TOPK + 1]
+    mixing = [v / (raised[0] + raised[1]) * shared for v in raised]
     both = (picks[0] + picks[1]).astype(jnp.bfloat16)
     earlier = (
         lax.broadcasted_iota(jnp.int32, (rows, rows), 0) > lax.broadcasted_iota(jnp.int32, (rows, rows), 1)
@@ -446,7 +484,7 @@
                 stage[pl.ds(c * chunks + 2 * j + h, peers, stride=span), :] = part[
                     c * peers : (c + 1) * peers, h * LANES : (h + 1) * LANES
                 ]
-    there, back = scratch[:7], scratch[7:]
+    there, back = scratch[:8], scratch[8:]
     pack(there, device)
     pl.semaphore_wait(barrier, len(ring) + 1)
     exchange(there)
@@ -484,15 +522,15 @@
             axis=1,
         ).astype(jnp.bfloat16)
         cols = slice(2 * j * LANES, (2 * j + 2) * LANES)
-        added = mix_ref[:, 0:1] * jnp.dot(chosen[0], block, preferred_element_type=jnp.float32) + mix_ref[
-            :, 1:2
+        added = mixing[0] * jnp.dot(chosen[0], block, preferred_element_type=jnp.float32) + mixing[
+            1
         ] * jnp.dot(chosen[1], block, preferred_element_type=jnp.float32)
         out_ref[:, cols] = (stream_ref[:, cols].astype(jnp.float32) + added).astype(jnp.bfloat16)
     sent(there)
     sent(back)
 
 
-def routed_experts(sp_n, tp_n, normed, stream, routes, mixing, w_gate, w_up, w_down):
+def routed_experts(sp_n, tp_n, normed, stream, small, w_gate, w_up, w_down):
     rows, width = normed.shape
     peers = sp_n * tp_n
     chips = sp_n // 2
@@ -506,12 +544,12 @@
 
     buffers = [
         blocks(2, chips * tp_n), blocks(chips * tp_n), blocks(tp_n, chips), blocks(chips, tp_n), blocks(chips, tp_n),
-        blocks(tp_n, chips), dma((10,)),
+        blocks(tp_n, chips), dma((PARTS, 8)), dma((2,)),
     ]
     return pl.pallas_call(
         functools.partial(moe_kernel, sp_n, tp_n),
         out_shape=jax.ShapeDtypeStruct((rows, width), jnp.bfloat16),
-        in_specs=[vmem] * 4 + [hbm] * 3,
+        in_specs=[vmem] * 3 + [hbm] * 3,
         out_specs=vmem,
         scratch_shapes=[
             pltpu.VMEM(w_gate.shape, jnp.bfloat16),
@@ -525,7 +563,7 @@
         ],
         compiler_params=pltpu.CompilerParams(collective_id=1, has_side_effects=True),
         name="routed_experts",
-    )(normed, stream, routes, mixing, w_gate, w_up, w_down)
+    )(normed, stream, small, w_gate, w_up, w_down)
 
 
 def shards(
@@ -560,16 +598,13 @@
         residual.reshape(row_count, D),
         norm_gain.reshape(1, D),
     )
-    mixing = jax.nn.softmax(pair_logits.reshape(row_count, TOPK), axis=-1) * group_prob.reshape(
-        row_count, 1
-    )
+    small = jnp.concatenate([routes.astype(jnp.float32), pair_logits, group_prob[..., None]], axis=-1)
     combined = routed_experts(
         lax.axis_size("sp"),
         lax.axis_size("tp"),
         normed,
         stream,
-        routes.reshape(row_count, TOPK),
-        mixing,
+        small.reshape(row_count, 2 * TOPK + 1),
         w_gate[0],
         w_up[0],
         w_down[0],

time: 158 us -> 143 us (0.905)
  Pallas kernels: 146 us -> 133 us
    pallas_call x1, Pallas kernels: 73.6 us -> 66.9 us  [routed_experts(): pl.pallas_call(functools.partial(moe_kernel, sp_n, tp_n), out_shape=jax.S...]
    pallas_call x1, Pallas kernels: 72.2 us -> 65.9 us  [attention(): pl.pallas_call(functools.partial(attention_kernel, sp_n, tp_n, seqs), out...]
where the time goes in v4:
time: 143 us
  Pallas kernels  133 us (93%)
  local copies, waits for them, and re-layouts  6.32 us (4%)
  other arithmetic  3.01 us (2%)
    pallas_call x1, Pallas kernels, routed_experts(): pl.pallas_call(functools.partial(moe_kernel, sp_n, tp_n), out_shape=jax.S...  66.9 us
    pallas_call x1, Pallas kernels, attention(): pl.pallas_call(functools.partial(attention_kernel, sp_n, tp_n, seqs), out...  65.9 us

profile of v4, /device:TPU:513, one launch (start us, length us, event | category | flops | bytes accessed | tf_op | source)
XLA Modules:
  0.0 143.2 jit_solution(7814179226216028669)
XLA Ops:
  0.0 1.1 copy.50
  1.1 0.4 multiply_cosine_fusion
  1.5 1.0 copy.60
  2.6 0.4 subtract_convert_fusion
  3.0 0.0 copy-start.1
  3.0 0.1 fusion.23
  3.2 0.8 fusion.20.q_ref
  4.0 0.1 copy-done.1
  4.1 0.3 fusion
  4.4 0.4 convolution_convert_fusion
  4.9 0.0 copy-done.6
  4.9 0.4 convolution_convert_fusion.1
  5.4 0.9 fusion.15.kv_ref
  6.3 0.8 reshape.89.res_ref
  7.1 65.9 %attention.1 = (bf16[96,2048]{1,0:T(8,128)(2,1)}, bf16[96,2048]{1,0:T(8,128)(2,1)}) custom-call(bf16[4,288,128]{2,1,0:T(8,128)(2,1)} %fusion.20.q_ref, bf16[4,480,128]{2,1,0:T(8,128)(2,1)} %fusion.15.kv_ref, bf16[128,2048]{1,0:T(8,128)(2,1)} %ow_ref.1, bf16[96,2048]{1,0:T(8,128)(2,1)} %reshape.89.res_ref, f32[1,2048]{1,0:T(1,128)} %bitcast.35), custom_call_target="tpu_custom_call" | custom-call | tf_op jit(solution)/shard_map/attention/pallas_call | solution.py:276
  73.1 0.1 copy.53
  73.2 0.1 concatenate.38
  73.3 0.1 copy.52
  73.4 0.1 concatenate.37
  73.5 0.1 copy.51
  73.6 0.1 concatenate.36
  73.7 0.7 copy.54.small_ref
  74.4 66.9 %routed_experts.1 = bf16[96,2048]{1,0:T(8,128)(2,1)} custom-call(bf16[96,2048]{1,0:T(8,128)(2,1)} %get-tuple-element.7.normed_ref, bf16[96,2048]{1,0:T(8,128)(2,1)} %get-tuple-element.8.stream_ref, f32[96,5]{1,0:T(8,128)} %copy.54.small_ref, bf16[2048,768]{1,0:T(8,128)(2,1)} %bitcast.30, bf16[2048,768]{1,0:T(8,128)(2,1)} %bitcast.31, bf16[768,2048]{1,0:T(8,128)(2,1)} %bitcast.32), custom_call_target="tpu_custom_call" | custom-call | tf_op jit(solution)/shard_map/routed_experts/pallas_call | solution.py:549
  141.3 1.9 %reshape.91 = bf16[24,4,2048]{2,1,0:T(4,128)(2,1)} reshape(bf16[96,2048]{1,0:T(8,128)(2,1)} %routed_experts.1) | data formatting | bytes 786432 | tf_op jit(solution)/shard_map/reshape | solution.py:612
  (20 shorter events, 0.1 us)
Async XLA Ops:
  0.0 4.4 %copy-start = (bf16[512,128]{1,0:T(8,128)(2,1)S(1)}, bf16[512,128]{1,0:T(8,128)(2,1)}, u32[]{:S(2)}) copy-start(bf16[512,128]{1,0:T(8,128)(2,1)} %param.21) | copy-start | bytes 393220
  3.0 1.1 copy-start.1
  3.0 1.4 %copy-start.7 = (f32[512]{0:T(512)S(1)}, f32[512]{0:T(512)}, u32[]{:S(2)}) copy-start(f32[512]{0:T(512)} %param.19) | copy-start | bytes 6148
  4.0 0.9 copy-start.6
  4.9 1.4 copy-start.2
  6.3 66.8 %copy-start.5 = (f32[24,4]{0,1:T(4,128)S(1)}, f32[24,4]{0,1:T(4,128)}, u32[]{:S(2)}) copy-start(f32[24,4]{0,1:T(4,128)} %param.24) | copy-start | bytes 1156
  6.3 67.0 %copy-start.3 = (f32[24,4,2]{0,2,1:T(2,128)S(1)}, f32[24,4,2]{0,2,1:T(2,128)}, u32[]{:S(2)}) copy-start(f32[24,4,2]{0,2,1:T(2,128)} %param.25) | copy-start | bytes 2308
  6.3 67.2 %copy-start.4 = (s32[24,4,2]{0,2,1:T(2,128)S(1)}, s32[24,4,2]{0,2,1:T(2,128)}, u32[]{:S(2)}) copy-start(s32[24,4,2]{0,2,1:T(2,128)} %param.26) | copy-start | bytes 2308

commit v5 on v4

--- a/solution.py
+++ b/solution.py
@@ -13,7 +13,6 @@
 QK = 192
 TOPK = 2
 CAP = 2
-PARTS = 2
 LANES = 128
 MESH = pl.DeviceIdType.MESH
 
@@ -313,7 +312,7 @@
 
 
 def moe_kernel(sp_n, tp_n, normed_ref, stream_ref, small_ref, wg_hbm, wu_hbm, wd_hbm, out_ref,
-               wg, wu, wd, stage, rows_in, w_sems, *scratch):
+               wg, wu, wd, stage, rows_in, sums, w_sems, *scratch):
     chips = sp_n // 2
     peers = sp_n * tp_n
     plane = chips * tp_n
@@ -357,102 +356,107 @@
     def landed(buffer, sem):
         pltpu.make_async_copy(buffer, buffer, sem).wait()
 
-    piece = span // PARTS
-
-    def exchange(buffers):
+    def part(p):
+        return pl.ds(p * chunks, chunks)
+
+    def begin(buffers, p):
         held, given, by_tp, by_sp, from_even, from_odd, sems, swap = buffers
-
-        def part(p):
-            return pl.ds(p * piece, piece)
-
-        def even_first():
-            for p in range(PARTS):
-                for way, d in ring:
-                    if way is across:
-                        to, where = across(d)
-                        src = held.at[0, pl.ds(to * chips, chips), part(p)]
-                        send(src, by_tp.at[tp, :, part(p)], sems.at[p, 0], sems.at[p, 1], where)
-
-        def odd_first():
-            for p in range(PARTS):
-                for way, d in ring:
-                    if way is along:
-                        to, where = along(d)
-                        src = held.at[1, pl.ds(to * tp_n, tp_n), part(p)]
-                        send(src, by_sp.at[chip, :, part(p)], sems.at[p, 2], sems.at[p, 3], where)
-
-        send(given, held.at[core], swap.at[0], swap.at[1], sibling)
-        pl.when(core == 0)(even_first)
-        pl.when(core == 1)(odd_first)
-        landed(given, swap.at[1])
-        pl.when(core == 1)(even_first)
-        pl.when(core == 0)(odd_first)
-        by_tp[tp] = held[0, pl.ds(tp * chips, chips)]
-        by_sp[chip] = held[1, pl.ds(chip * tp_n, tp_n)]
-        for p in range(PARTS):
-            landed(by_tp.at[pl.ds(0, tp_n - 1), :, part(p)], sems.at[p, 1])
-            for way, d in ring:
-                if way is along:
-                    to, where = along(d)
-                    send(by_tp.at[:, to, part(p)], from_even.at[chip, :, part(p)], sems.at[p, 4], sems.at[p, 5], where)
-            landed(by_sp.at[pl.ds(0, chips - 1), :, part(p)], sems.at[p, 3])
-            for way, d in ring:
-                if way is across:
-                    to, where = across(d)
-                    send(by_sp.at[:, to, part(p)], from_odd.at[tp, :, part(p)], sems.at[p, 6], sems.at[p, 7], where)
-        from_even[chip] = by_tp[:, chip]
-        from_odd[tp] = by_sp[:, tp]
-        for p in range(PARTS):
-            landed(from_even.at[pl.ds(0, chips - 1), :, part(p)], sems.at[p, 5])
-            landed(from_odd.at[pl.ds(0, tp_n - 1), :, part(p)], sems.at[p, 7])
+        send(given.at[:, part(p)], held.at[core, :, part(p)], swap.at[p, 0], swap.at[p, 1], sibling)
+        pl.when(core == 0)(functools.partial(even_first, buffers, p))
+        pl.when(core == 1)(functools.partial(odd_first, buffers, p))
+
+    def even_first(buffers, p):
+        held, given, by_tp, by_sp, from_even, from_odd, sems, swap = buffers
+        for way, d in ring:
+            if way is across:
+                to, where = across(d)
+                src = held.at[0, pl.ds(to * chips, chips), part(p)]
+                send(src, by_tp.at[tp, :, part(p)], sems.at[p, 0], sems.at[p, 1], where)
+
+    def odd_first(buffers, p):
+        held, given, by_tp, by_sp, from_even, from_odd, sems, swap = buffers
+        for way, d in ring:
+            if way is along:
+                to, where = along(d)
+                src = held.at[1, pl.ds(to * tp_n, tp_n), part(p)]
+                send(src, by_sp.at[chip, :, part(p)], sems.at[p, 2], sems.at[p, 3], where)
+
+    def rest(buffers, p):
+        held, given, by_tp, by_sp, from_even, from_odd, sems, swap = buffers
+        landed(given.at[:, part(p)], swap.at[p, 1])
+        pl.when(core == 1)(functools.partial(even_first, buffers, p))
+        pl.when(core == 0)(functools.partial(odd_first, buffers, p))
+        by_tp[tp, :, part(p)] = held[0, pl.ds(tp * chips, chips), part(p)]
+        by_sp[chip, :, part(p)] = held[1, pl.ds(chip * tp_n, tp_n), part(p)]
+
+    def turn(buffers, p):
+        held, given, by_tp, by_sp, from_even, from_odd, sems, swap = buffers
+        landed(by_tp.at[pl.ds(0, tp_n - 1), :, part(p)], sems.at[p, 1])
+        for way, d in ring:
+            if way is along:
+                to, where = along(d)
+                send(by_tp.at[:, to, part(p)], from_even.at[chip, :, part(p)], sems.at[p, 4], sems.at[p, 5], where)
+        landed(by_sp.at[pl.ds(0, chips - 1), :, part(p)], sems.at[p, 3])
+        for way, d in ring:
+            if way is across:
+                to, where = across(d)
+                send(by_sp.at[:, to, part(p)], from_odd.at[tp, :, part(p)], sems.at[p, 6], sems.at[p, 7], where)
+        from_even[chip, :, part(p)] = by_tp[:, chip, part(p)]
+        from_odd[tp, :, part(p)] = by_sp[:, tp, part(p)]
+
+    def finish(buffers, p):
+        held, given, by_tp, by_sp, from_even, from_odd, sems, swap = buffers
+        landed(from_even.at[pl.ds(0, chips - 1), :, part(p)], sems.at[p, 5])
+        landed(from_odd.at[pl.ds(0, tp_n - 1), :, part(p)], sems.at[p, 7])
 
     def sent(buffers):
         held, given, by_tp, by_sp, from_even, from_odd, sems, swap = buffers
-        landed(given, swap.at[0])
-        for p in range(PARTS):
-            part = pl.ds(p * piece, piece)
-            landed(by_tp.at[pl.ds(0, tp_n - 1), :, part], sems.at[p, 0])
-            landed(by_sp.at[pl.ds(0, chips - 1), :, part], sems.at[p, 2])
-            landed(from_even.at[pl.ds(0, chips - 1), :, part], sems.at[p, 4])
-            landed(from_odd.at[pl.ds(0, tp_n - 1), :, part], sems.at[p, 6])
+        for p in range(CAP):
+            landed(given.at[:, part(p)], swap.at[p, 0])
+            landed(by_tp.at[pl.ds(0, tp_n - 1), :, part(p)], sems.at[p, 0])
+            landed(by_sp.at[pl.ds(0, chips - 1), :, part(p)], sems.at[p, 2])
+            landed(from_even.at[pl.ds(0, chips - 1), :, part(p)], sems.at[p, 4])
+            landed(from_odd.at[pl.ds(0, tp_n - 1), :, part(p)], sems.at[p, 6])
+
+    def device(c, core_id, x):
+        return (2 * c + core_id) * tp_n + x
 
     step = min(8, plane)
 
-    def pack(buffers, place):
+    def pack(buffers, p):
         held, given = buffers[:2]
 
         def block(i, to_core):
             c = lax.rem(i, chips) * (1 - core) + i // tp_n * core
             x = i // chips * (1 - core) + lax.rem(i, tp_n) * core
-            return stage[pl.ds(pl.multiple_of(place(c, to_core, x) * span, span), span), :].astype(jnp.bfloat16)
+            start = pl.multiple_of(device(c, to_core, x) * span, span) + p * chunks
+            return stage[pl.ds(start, chunks), :].astype(jnp.bfloat16)
 
         def body(n, _):
             for j in range(step):
                 i = n * step + j
-                held[core, i] = block(i, core)
-                given[i] = block(i, 1 - core)
+                held[core, i, part(p)] = block(i, core)
+                given[i, part(p)] = block(i, 1 - core)
             return 0
 
         lax.fori_loop(0, plane // step, body, 0)
 
-    def unpack(buffers, place):
+    def unpack(buffers, p):
         from_even, from_odd = buffers[4:6]
 
         def put(where, block):
-            stage[pl.ds(pl.multiple_of(where * span, span), span), :] = block.astype(jnp.float32)
+            start = pl.multiple_of(where * span, span) + p * chunks
+            stage[pl.ds(start, chunks), :] = block.astype(jnp.float32)
 
         def body(n, _):
             for j in range(step):
                 i = n * step + j
                 c, x = i // tp_n, lax.rem(i, tp_n)
-                put(place(c, 0, x), from_even[c, x])
-                put(place(c, 1, x), from_odd[x, c])
+                put(device(c, 0, x), from_even[c, x, part(p)])
+                put(device(c, 1, x), from_odd[x, c, part(p)])
             return 0
 
         lax.fori_loop(0, plane // step, body, 0)
-
-    def device(c, core_id, x):
-        return (2 * c + core_id) * tp_n + x
 
     experts = lax.broadcasted_iota(jnp.int32, (rows, peers), 1).astype(jnp.float32)
     small = small_ref[...]
@@ -475,57 +479,73 @@
     chosen = [c.astype(jnp.bfloat16) for c in chosen]
 
     for j in range(chunks // 2):
-        part = lax.dot_general(
+        placed = lax.dot_general(
             taken, normed_ref[:, 2 * j * LANES : (2 * j + 2) * LANES], (((0,), (0,)), ((), ())),
             preferred_element_type=jnp.float32,
         )
         for c in range(CAP):
             for h in range(2):
-                stage[pl.ds(c * chunks + 2 * j + h, peers, stride=span), :] = part[
+                stage[pl.ds(c * chunks + 2 * j + h, peers, stride=span), :] = placed[
                     c * peers : (c + 1) * peers, h * LANES : (h + 1) * LANES
                 ]
     there, back = scratch[:8], scratch[8:]
-    pack(there, device)
+    for p in range(CAP):
+        pack(there, p)
     pl.semaphore_wait(barrier, len(ring) + 1)
-    exchange(there)
+    for p in range(CAP):
+        begin(there, p)
+    for p in range(CAP):
+        rest(there, p)
+    for p in range(CAP):
+        turn(there, p)
     for load in loads:
         load.wait()
 
-    unpack(there, device)
-    total = peers * CAP
-    for l in range(chunks):
-        rows_in[:, l * LANES : (l + 1) * LANES] = stage[pl.ds(l, total, stride=chunks), :].astype(jnp.bfloat16)
     tile = 256
-    hidden = []
-    for j in range(wg.shape[1] // tile):
-        cols = slice(j * tile, (j + 1) * tile)
-        gate = jnp.dot(rows_in[...], wg[:, cols], preferred_element_type=jnp.float32)
-        up = jnp.dot(rows_in[...], wu[:, cols], preferred_element_type=jnp.float32)
-        hidden.append((gate / (1.0 + jnp.exp(-gate)) * up).astype(jnp.bfloat16))
-    hidden = jnp.concatenate(hidden, axis=1)
-    for j in range(chunks // 2):
-        part = jnp.dot(hidden, wd[:, 2 * j * LANES : (2 * j + 2) * LANES], preferred_element_type=jnp.float32)
-        for h in range(2):
-            stage[pl.ds(2 * j + h, total, stride=chunks), :] = part[:, h * LANES : (h + 1) * LANES]
-    pack(back, device)
-    exchange(back)
-
-    unpack(back, device)
-    for j in range(chunks // 2):
-        block = jnp.concatenate(
-            [
-                jnp.concatenate(
-                    [stage[pl.ds(c * chunks + 2 * j + h, peers, stride=span), :] for c in range(CAP)], axis=0
-                )
-                for h in range(2)
-            ],
-            axis=1,
-        ).astype(jnp.bfloat16)
-        cols = slice(2 * j * LANES, (2 * j + 2) * LANES)
-        added = mixing[0] * jnp.dot(chosen[0], block, preferred_element_type=jnp.float32) + mixing[
-            1
-        ] * jnp.dot(chosen[1], block, preferred_element_type=jnp.float32)
-        out_ref[:, cols] = (stream_ref[:, cols].astype(jnp.float32) + added).astype(jnp.bfloat16)
+
+    def serve(p):
+        for l in range(chunks):
+            rows_in[:, l * LANES : (l + 1) * LANES] = stage[pl.ds(p * chunks + l, peers, stride=span), :].astype(
+                jnp.bfloat16
+            )
+        hidden = []
+        for j in range(wg.shape[1] // tile):
+            cols = slice(j * tile, (j + 1) * tile)
+            gate = jnp.dot(rows_in[...], wg[:, cols], preferred_element_type=jnp.float32)
+            up = jnp.dot(rows_in[...], wu[:, cols], preferred_element_type=jnp.float32)
+            hidden.append((gate / (1.0 + jnp.exp(-gate)) * up).astype(jnp.bfloat16))
+        hidden = jnp.concatenate(hidden, axis=1)
+        for j in range(chunks // 2):
+            out = jnp.dot(hidden, wd[:, 2 * j * LANES : (2 * j + 2) * LANES], preferred_element_type=jnp.float32)
+            for h in range(2):
+                stage[pl.ds(p * chunks + 2 * j + h, peers, stride=span), :] = out[:, h * LANES : (h + 1) * LANES]
+
+    for p in range(CAP):
+        finish(there, p)
+        unpack(there, p)
+        serve(p)
+        pack(back, p)
+        begin(back, p)
+        rest(back, p)
+    for p in range(CAP):
+        turn(back, p)
+
+    for p in range(CAP):
+        finish(back, p)
+        unpack(back, p)
+        for j in range(chunks // 2):
+            block = jnp.concatenate(
+                [stage[pl.ds(p * chunks + 2 * j + h, peers, stride=span), :] for h in range(2)], axis=1
+            ).astype(jnp.bfloat16)
+            cols = slice(2 * j * LANES, (2 * j + 2) * LANES)
+            added = 0.0 if p == 0 else sums[:, cols]
+            for k in range(TOPK):
+                picked = chosen[k][:, p * peers : (p + 1) * peers]
+                added = added + mixing[k] * jnp.dot(picked, block, preferred_element_type=jnp.float32)
+            if p < CAP - 1:
+                sums[:, cols] = added
+            else:
+                out_ref[:, cols] = (stream_ref[:, cols].astype(jnp.float32) + added).astype(jnp.bfloat16)
     sent(there)
     sent(back)
 
@@ -544,7 +564,7 @@
 
     buffers = [
         blocks(2, chips * tp_n), blocks(chips * tp_n), blocks(tp_n, chips), blocks(chips, tp_n), blocks(chips, tp_n),
-        blocks(tp_n, chips), dma((PARTS, 8)), dma((2,)),
+        blocks(tp_n, chips), dma((CAP, 8)), dma((CAP, 2)),
     ]
     return pl.pallas_call(
         functools.partial(moe_kernel, sp_n, tp_n),
@@ -556,7 +576,8 @@
             pltpu.VMEM(w_up.shape, jnp.bfloat16),
             pltpu.VMEM(w_down.shape, jnp.bfloat16),
             pltpu.VMEM((peers * span, LANES), jnp.float32),
-            pltpu.VMEM((peers * CAP, width), jnp.bfloat16),
+            pltpu.VMEM((peers, width), jnp.bfloat16),
+            pltpu.VMEM((rows, width), jnp.float32),
             dma((3,)),
             *buffers,
             *buffers,

time: 143 us -> 138 us (0.965)
  Pallas kernels: 133 us -> 127 us
    pallas_call x1, Pallas kernels: 66.9 us -> 61.2 us  [routed_experts(): pl.pallas_call(functools.partial(moe_kernel, sp_n, tp_n), out_shape=jax.S...]
where the time goes in v5:
time: 138 us
  Pallas kernels  127 us (92%)
  local copies, waits for them, and re-layouts  6.32 us (5%)
  other arithmetic  3.01 us (2%)
    pallas_call x1, Pallas kernels, attention(): pl.pallas_call(functools.partial(attention_kernel, sp_n, tp_n, seqs), out...  65.9 us
    pallas_call x1, Pallas kernels, routed_experts(): pl.pallas_call(functools.partial(moe_kernel, sp_n, tp_n), out_shape=jax.S...  61.2 us

profile of v5, /device:TPU:513, one launch (start us, length us, event | category | flops | bytes accessed | tf_op | source)
XLA Modules:
  0.0 137.5 jit_solution(11125028242684567719)
XLA Ops:
  0.0 1.1 copy.50
  1.1 0.4 multiply_cosine_fusion
  1.5 1.0 copy.60
  2.6 0.4 subtract_convert_fusion
  3.0 0.0 copy-start.1
  3.0 0.1 fusion.23
  3.2 0.8 fusion.20.q_ref
  4.0 0.1 copy-done.1
  4.1 0.3 fusion
  4.4 0.4 convolution_convert_fusion
  4.9 0.0 copy-done.6
  4.9 0.4 convolution_convert_fusion.1
  5.4 0.9 fusion.15.kv_ref
  6.3 0.8 reshape.89.res_ref
  7.1 65.9 %attention.1 = (bf16[96,2048]{1,0:T(8,128)(2,1)}, bf16[96,2048]{1,0:T(8,128)(2,1)}) custom-call(bf16[4,288,128]{2,1,0:T(8,128)(2,1)} %fusion.20.q_ref, bf16[4,480,128]{2,1,0:T(8,128)(2,1)} %fusion.15.kv_ref, bf16[128,2048]{1,0:T(8,128)(2,1)} %ow_ref.1, bf16[96,2048]{1,0:T(8,128)(2,1)} %reshape.89.res_ref, f32[1,2048]{1,0:T(1,128)} %bitcast.35), custom_call_target="tpu_custom_call" | custom-call | tf_op jit(solution)/shard_map/attention/pallas_call | solution.py:275
  73.1 0.1 copy.53
  73.2 0.1 concatenate.38
  73.3 0.1 copy.52
  73.4 0.1 concatenate.37
  73.5 0.1 copy.51
  73.6 0.1 concatenate.36
  73.7 0.7 copy.54.small_ref
  74.4 61.2 %routed_experts.1 = bf16[96,2048]{1,0:T(8,128)(2,1)} custom-call(bf16[96,2048]{1,0:T(8,128)(2,1)} %get-tuple-element.7.normed_ref, bf16[96,2048]{1,0:T(8,128)(2,1)} %get-tuple-element.8.stream_ref, f32[96,5]{1,0:T(8,128)} %copy.54.small_ref, bf16[2048,768]{1,0:T(8,128)(2,1)} %bitcast.30, bf16[2048,768]{1,0:T(8,128)(2,1)} %bitcast.31, bf16[768,2048]{1,0:T(8,128)(2,1)} %bitcast.32), custom_call_target="tpu_custom_call" | custom-call | tf_op jit(solution)/shard_map/routed_experts/pallas_call | solution.py:569
  135.6 1.9 %reshape.91 = bf16[24,4,2048]{2,1,0:T(4,128)(2,1)} reshape(bf16[96,2048]{1,0:T(8,128)(2,1)} %routed_experts.1) | data formatting | bytes 786432 | tf_op jit(solution)/shard_map/reshape | solution.py:633
  (20 shorter events, 0.1 us)
Async XLA Ops:
  0.0 4.4 %copy-start = (bf16[512,128]{1,0:T(8,128)(2,1)S(1)}, bf16[512,128]{1,0:T(8,128)(2,1)}, u32[]{:S(2)}) copy-start(bf16[512,128]{1,0:T(8,128)(2,1)} %param.21) | copy-start | bytes 393220
  3.0 1.1 copy-start.1
  3.0 1.4 %copy-start.7 = (f32[512]{0:T(512)S(1)}, f32[512]{0:T(512)}, u32[]{:S(2)}) copy-start(f32[512]{0:T(512)} %param.19) | copy-start | bytes 6148
  4.0 0.9 copy-start.6
  4.9 1.4 copy-start.2
  6.3 66.8 %copy-start.5 = (f32[24,4]{0,1:T(4,128)S(1)}, f32[24,4]{0,1:T(4,128)}, u32[]{:S(2)}) copy-start(f32[24,4]{0,1:T(4,128)} %param.24) | copy-start | bytes 1156
  6.3 67.0 %copy-start.3 = (f32[24,4,2]{0,2,1:T(2,128)S(1)}, f32[24,4,2]{0,2,1:T(2,128)}, u32[]{:S(2)}) copy-start(f32[24,4,2]{0,2,1:T(2,128)} %param.25) | copy-start | bytes 2308
  6.3 67.2 %copy-start.4 = (s32[24,4,2]{0,2,1:T(2,128)S(1)}, s32[24,4,2]{0,2,1:T(2,128)}, u32[]{:S(2)}) copy-start(s32[24,4,2]{0,2,1:T(2,128)} %param.26) | copy-start | bytes 2308

commit v6 on v5

--- a/solution.py
+++ b/solution.py
@@ -93,7 +93,7 @@
     pl.semaphore_wait(barrier, len(peers))
 
     own_slot = slot(core, own_g, 0)
-    for seq, g, home, k in homes:
+    for seq, g, home, k in homes[1:2] + homes[:1] + homes[2:]:
         send(kv_ref.at[seq], kv_all.at[slot(core, g, k)], kv_sent, kv_sem.at[k], at(home))
 
     def ow_stage(r):
@@ -478,23 +478,22 @@
     taken = (chosen[0] + chosen[1]).astype(jnp.bfloat16)
     chosen = [c.astype(jnp.bfloat16) for c in chosen]
 
-    for j in range(chunks // 2):
-        placed = lax.dot_general(
-            taken, normed_ref[:, 2 * j * LANES : (2 * j + 2) * LANES], (((0,), (0,)), ((), ())),
-            preferred_element_type=jnp.float32,
-        )
-        for c in range(CAP):
-            for h in range(2):
-                stage[pl.ds(c * chunks + 2 * j + h, peers, stride=span), :] = placed[
-                    c * peers : (c + 1) * peers, h * LANES : (h + 1) * LANES
-                ]
     there, back = scratch[:8], scratch[8:]
     for p in range(CAP):
+        for j in range(chunks // 2):
+            placed = lax.dot_general(
+                taken[:, p * peers : (p + 1) * peers], normed_ref[:, 2 * j * LANES : (2 * j + 2) * LANES],
+                (((0,), (0,)), ((), ())), preferred_element_type=jnp.float32,
+            )
+            for h in range(2):
+                stage[pl.ds(p * chunks + 2 * j + h, peers, stride=span), :] = placed[:, h * LANES : (h + 1) * LANES]
         pack(there, p)
-    pl.semaphore_wait(barrier, len(ring) + 1)
-    for p in range(CAP):
+        if p == 0:
+            pl.semaphore_wait(barrier, len(ring) + 1)
         begin(there, p)
-    for p in range(CAP):
+        if p == 0:
+            rest(there, p)
+    for p in range(1, CAP):
         rest(there, p)
     for p in range(CAP):
         turn(there, p)

time: 138 us -> 138 us (level)
  no operation moved by 1% of the time
where the time goes in v6:
time: 138 us
  Pallas kernels  127 us (92%)
  local copies, waits for them, and re-layouts  6.32 us (5%)
  other arithmetic  3.01 us (2%)
    pallas_call x1, Pallas kernels, attention(): pl.pallas_call(functools.partial(attention_kernel, sp_n, tp_n, seqs), out...  66.4 us
    pallas_call x1, Pallas kernels, routed_experts(): pl.pallas_call(functools.partial(moe_kernel, sp_n, tp_n), out_shape=jax.S...  60.8 us

profile of v6, /device:TPU:513, one launch (start us, length us, event | category | flops | bytes accessed | tf_op | source)
XLA Modules:
  0.0 137.5 jit_solution(2268417767661103164)
XLA Ops:
  0.0 1.1 copy.50
  1.1 0.4 multiply_cosine_fusion
  1.5 1.0 copy.60
  2.6 0.4 subtract_convert_fusion
  3.0 0.0 copy-start.1
  3.0 0.1 fusion.23
  3.2 0.8 fusion.20.q_ref
  4.0 0.1 copy-done.1
  4.1 0.3 fusion
  4.4 0.4 convolution_convert_fusion
  4.9 0.0 copy-done.6
  4.9 0.4 convolution_convert_fusion.1
  5.4 0.9 fusion.15.kv_ref
  6.3 0.8 reshape.89.res_ref
  7.1 66.4 %attention.1 = (bf16[96,2048]{1,0:T(8,128)(2,1)}, bf16[96,2048]{1,0:T(8,128)(2,1)}) custom-call(bf16[4,288,128]{2,1,0:T(8,128)(2,1)} %fusion.20.q_ref, bf16[4,480,128]{2,1,0:T(8,128)(2,1)} %fusion.15.kv_ref, bf16[128,2048]{1,0:T(8,128)(2,1)} %ow_ref.1, bf16[96,2048]{1,0:T(8,128)(2,1)} %reshape.89.res_ref, f32[1,2048]{1,0:T(1,128)} %bitcast.35), custom_call_target="tpu_custom_call" | custom-call | tf_op jit(solution)/shard_map/attention/pallas_call | solution.py:275
  73.5 0.1 copy.53
  73.6 0.1 concatenate.38
  73.7 0.1 copy.52
  73.8 0.1 concatenate.37
  73.9 0.1 copy.51
  74.0 0.1 concatenate.36
  74.1 0.7 copy.54.small_ref
  74.8 60.8 %routed_experts.1 = bf16[96,2048]{1,0:T(8,128)(2,1)} custom-call(bf16[96,2048]{1,0:T(8,128)(2,1)} %get-tuple-element.7.normed_ref, bf16[96,2048]{1,0:T(8,128)(2,1)} %get-tuple-element.8.stream_ref, f32[96,5]{1,0:T(8,128)} %copy.54.small_ref, bf16[2048,768]{1,0:T(8,128)(2,1)} %bitcast.30, bf16[2048,768]{1,0:T(8,128)(2,1)} %bitcast.31, bf16[768,2048]{1,0:T(8,128)(2,1)} %bitcast.32), custom_call_target="tpu_custom_call" | custom-call | tf_op jit(solution)/shard_map/routed_experts/pallas_call | solution.py:568
  135.7 1.9 %reshape.91 = bf16[24,4,2048]{2,1,0:T(4,128)(2,1)} reshape(bf16[96,2048]{1,0:T(8,128)(2,1)} %routed_experts.1) | data formatting | bytes 786432 | tf_op jit(solution)/shard_map/reshape | solution.py:632
  (20 shorter events, 0.1 us)
Async XLA Ops:
  0.0 4.4 %copy-start = (bf16[512,128]{1,0:T(8,128)(2,1)S(1)}, bf16[512,128]{1,0:T(8,128)(2,1)}, u32[]{:S(2)}) copy-start(bf16[512,128]{1,0:T(8,128)(2,1)} %param.21) | copy-start | bytes 393220
  3.0 1.1 copy-start.1
  3.0 1.4 %copy-start.7 = (f32[512]{0:T(512)S(1)}, f32[512]{0:T(512)}, u32[]{:S(2)}) copy-start(f32[512]{0:T(512)} %param.19) | copy-start | bytes 6148
  4.0 0.9 copy-start.6
  4.9 1.4 copy-start.2
  6.3 67.2 %copy-start.5 = (f32[24,4]{0,1:T(4,128)S(1)}, f32[24,4]{0,1:T(4,128)}, u32[]{:S(2)}) copy-start(f32[24,4]{0,1:T(4,128)} %param.24) | copy-start | bytes 1156
  6.3 67.4 %copy-start.3 = (f32[24,4,2]{0,2,1:T(2,128)S(1)}, f32[24,4,2]{0,2,1:T(2,128)}, u32[]{:S(2)}) copy-start(f32[24,4,2]{0,2,1:T(2,128)} %param.25) | copy-start | bytes 2308
  6.3 67.6 %copy-start.4 = (s32[24,4,2]{0,2,1:T(2,128)S(1)}, s32[24,4,2]{0,2,1:T(2,128)}, u32[]{:S(2)}) copy-start(s32[24,4,2]{0,2,1:T(2,128)} %param.26) | copy-start | bytes 2308

commit v7 on v6

--- a/solution.py
+++ b/solution.py
@@ -544,12 +544,13 @@
             if p < CAP - 1:
                 sums[:, cols] = added
             else:
-                out_ref[:, cols] = (stream_ref[:, cols].astype(jnp.float32) + added).astype(jnp.bfloat16)
+                summed = stream_ref[:, cols].astype(jnp.float32) + added
+                out_ref[:, :, cols] = summed.reshape(*out_ref.shape[:2], 2 * LANES).astype(jnp.bfloat16)
     sent(there)
     sent(back)
 
 
-def routed_experts(sp_n, tp_n, normed, stream, small, w_gate, w_up, w_down):
+def routed_experts(sp_n, tp_n, shape, normed, stream, small, w_gate, w_up, w_down):
     rows, width = normed.shape
     peers = sp_n * tp_n
     chips = sp_n // 2
@@ -567,7 +568,7 @@
     ]
     return pl.pallas_call(
         functools.partial(moe_kernel, sp_n, tp_n),
-        out_shape=jax.ShapeDtypeStruct((rows, width), jnp.bfloat16),
+        out_shape=jax.ShapeDtypeStruct(shape, jnp.bfloat16),
         in_specs=[vmem] * 3 + [hbm] * 3,
         out_specs=vmem,
         scratch_shapes=[
@@ -619,9 +620,10 @@
         norm_gain.reshape(1, D),
     )
     small = jnp.concatenate([routes.astype(jnp.float32), pair_logits, group_prob[..., None]], axis=-1)
-    combined = routed_experts(
+    return routed_experts(
         lax.axis_size("sp"),
         lax.axis_size("tp"),
+        residual.shape,
         normed,
         stream,
         small.reshape(row_count, 2 * TOPK + 1),
@@ -629,7 +631,6 @@
         w_up[0],
         w_down[0],
     )
-    return combined.reshape(residual.shape)
 
 
 def solution(mesh):

time: 138 us -> 138 us (level)
    unnamed x19 -> x20, local copies, waits for them, and re-layouts: 1.39 us -> 3.29 us
    reshape x1 -> x0, local copies, waits for them, and re-layouts: 1.89 us -> none  [shards(): return combined.reshape(residual.shape)]
where the time goes in v7:
time: 138 us
  Pallas kernels  127 us (92%)
  local copies, waits for them, and re-layouts  6.34 us (5%)
  other arithmetic  3.01 us (2%)
    pallas_call x1, Pallas kernels, attention(): pl.pallas_call(functools.partial(attention_kernel, sp_n, tp_n, seqs), out...  66.4 us
    pallas_call x1, Pallas kernels, routed_experts(): pl.pallas_call(functools.partial(moe_kernel, sp_n, tp_n), out_shape=jax.S...  60.8 us
    unnamed x20, local copies, waits for them, and re-layouts  3.29 us

profile of v7, /device:TPU:513, one launch (start us, length us, event | category | flops | bytes accessed | tf_op | source)
XLA Modules:
  0.0 137.6 jit_solution(17219351825954761539)
XLA Ops:
  0.0 1.1 copy.50
  1.1 0.4 multiply_cosine_fusion
  1.5 1.0 copy.60
  2.6 0.4 subtract_convert_fusion
  3.0 0.0 copy-start.1
  3.0 0.1 fusion.23
  3.2 0.8 fusion.20.q_ref
  4.0 0.1 copy-done.1
  4.1 0.3 fusion
  4.4 0.4 convolution_convert_fusion
  4.9 0.0 copy-done.6
  4.9 0.4 convolution_convert_fusion.1
  5.4 0.9 fusion.15.kv_ref
  6.3 0.8 reshape.86.res_ref
  7.1 66.4 %attention.1 = (bf16[96,2048]{1,0:T(8,128)(2,1)}, bf16[96,2048]{1,0:T(8,128)(2,1)}) custom-call(bf16[4,288,128]{2,1,0:T(8,128)(2,1)} %fusion.20.q_ref, bf16[4,480,128]{2,1,0:T(8,128)(2,1)} %fusion.15.kv_ref, bf16[128,2048]{1,0:T(8,128)(2,1)} %ow_ref.1, bf16[96,2048]{1,0:T(8,128)(2,1)} %reshape.86.res_ref, f32[1,2048]{1,0:T(1,128)} %bitcast.35), custom_call_target="tpu_custom_call" | custom-call | tf_op jit(solution)/shard_map/attention/pallas_call | solution.py:275
  73.5 0.1 copy.53
  73.6 0.1 concatenate.38
  73.7 0.1 copy.52
  73.8 0.1 concatenate.37
  73.9 0.1 copy.51
  74.0 0.1 concatenate.36
  74.1 0.7 copy.54.small_ref
  74.8 60.8 %routed_experts.1 = bf16[24,4,2048]{2,1,0:T(4,128)(2,1)} custom-call(bf16[96,2048]{1,0:T(8,128)(2,1)} %get-tuple-element.7.normed_ref, bf16[96,2048]{1,0:T(8,128)(2,1)} %get-tuple-element.8.stream_ref, f32[96,5]{1,0:T(8,128)} %copy.54.small_ref, bf16[2048,768]{1,0:T(8,128)(2,1)} %bitcast.30, bf16[2048,768]{1,0:T(8,128)(2,1)} %bitcast.31, ...), custom_call_target="tpu_custom_call" | custom-call | tf_op jit(solution)/shard_map/routed_experts/pallas_call | solution.py:569
  135.7 1.9 %copy.62 = bf16[24,4,2048]{2,1,0:T(4,128)(2,1)} copy(bf16[24,4,2048]{2,1,0:T(4,128)(2,1)} %routed_experts.1) | data formatting | bytes 786432
  (20 shorter events, 0.1 us)
Async XLA Ops:
  0.0 4.4 %copy-start = (bf16[512,128]{1,0:T(8,128)(2,1)S(1)}, bf16[512,128]{1,0:T(8,128)(2,1)}, u32[]{:S(2)}) copy-start(bf16[512,128]{1,0:T(8,128)(2,1)} %param.21) | copy-start | bytes 393220
  3.0 1.1 copy-start.1
  3.0 1.4 %copy-start.7 = (f32[512]{0:T(512)S(1)}, f32[512]{0:T(512)}, u32[]{:S(2)}) copy-start(f32[512]{0:T(512)} %param.19) | copy-start | bytes 6148
  4.0 0.9 copy-start.6
  4.9 1.4 copy-start.2
  6.3 67.2 %copy-start.5 = (f32[24,4]{0,1:T(4,128)S(1)}, f32[24,4]{0,1:T(4,128)}, u32[]{:S(2)}) copy-start(f32[24,4]{0,1:T(4,128)} %param.24) | copy-start | bytes 1156
  6.3 67.4 %copy-start.3 = (f32[24,4,2]{0,2,1:T(2,128)S(1)}, f32[24,4,2]{0,2,1:T(2,128)}, u32[]{:S(2)}) copy-start(f32[24,4,2]{0,2,1:T(2,128)} %param.25) | copy-start | bytes 2308
  6.3 67.6 %copy-start.4 = (s32[24,4,2]{0,2,1:T(2,128)S(1)}, s32[24,4,2]{0,2,1:T(2,128)}, u32[]{:S(2)}) copy-start(s32[24,4,2]{0,2,1:T(2,128)} %param.26) | copy-start | bytes 2308
